TPU v7x, 512 devices: a whole 4x4x16 slice. The times are simulated.
512 devices in a mesh: kv: 16 (over y, x), tp: 32 (over z, core).
Axes of the slice: x: 4, y: 4, z: 16, core: 2. Of those that a mesh axis runs over, the one named last changes fastest.
Arguments:
- tokens: bfloat16 [64, 4096], P(None, ('kv', 'tp')), may hold values from -9 to 9
- lengths: int32 [64], replicated, may hold values from 1 to 16384, 262144 in all
- gain_attn: float32 [4096], P('kv'), may hold values from 0.1 to 1.9
- w_query_nope: bfloat16 [4096, 4096], P('kv', 'tp'), may hold values from -0.09375 to 0.09375
- w_query_rope: bfloat16 [4096, 2048], P('kv', 'tp'), may hold values from -0.09375 to 0.09375
- w_latent: bfloat16 [4096, 512], P('kv'), may hold values from -0.09375 to 0.09375
- w_rope_key: bfloat16 [4096, 64], P('kv'), may hold values from -0.09375 to 0.09375
- gain_latent: float32 [512], replicated, may hold values from 0.1 to 1.9
- w_key_up: bfloat16 [512, 4096], P(None, 'tp'), may hold values from -0.75 to 0.75
- w_value_up: bfloat16 [512, 4096], P(None, 'tp'), may hold values from -0.25 to 0.25
- w_out: bfloat16 [4096, 4096], P('tp', 'kv'), may hold values from -0.25 to 0.25
- gain_mlp: float32 [4096], P('kv'), may hold values from 0.1 to 1.9
- w_up: bfloat16 [4096, 16384], P('kv', 'tp'), may hold values from -0.09375 to 0.09375
- w_down: bfloat16 [16384, 4096], P('tp', 'kv'), may hold values from -0.046875 to 0.046875
- cache_latent: bfloat16 [64, 16384, 512], P('tp', 'kv'), may hold values from -6 to 6
- cache_rope: bfloat16 [64, 16384, 64], P('tp', 'kv'), may hold values from -900 to 900
Outputs:
- mixed: bfloat16 [64, 4096], P(None, ('kv', 'tp'))
Inputs may be any that keep to these rules, and one draw needn't show every extreme that they name: `lengths`: one sequence has exactly 16384 live positions.
All inputs are finite; a program needn't handle non-finite values.
Results may differ from a plain program's by a relative error of at most 0.035.
The roundings to bfloat16 on the way count: a program that leaves them out, or rounds other values in their place, can miss the bound.
Values may be sent and summed in bfloat16 or wider, within the bound.
No kernel may reach another device: no remote copies, remote signals or barrier semaphores. Data moves between devices by JAX's collectives and lax.ppermute only.
A program may use at most 64 MiB of HBM per device.

v0:
```python
import jax
import jax.numpy as jnp
from jax import lax
from jax.sharding import Mesh
from jax.sharding import PartitionSpec as P

D = 4096
NOPE = 128
ROPE = 64
VD = 128
RANK = 512
KV = ("kv_0", "kv_1")
KV_TP = ("kv_0", "kv_1", "tp")


EPS = 1e-06


def in_order(parts, dim):
    parts = jnp.moveaxis(parts, 0, dim)
    dims = parts.shape
    return parts.reshape(*dims[:dim], dims[dim] * dims[dim + 1], *dims[dim + 2 :])


def sent_to_all(value, axis):
    peers = lax.axis_size(axis)
    return lax.all_to_all(
        jnp.broadcast_to(value[None], (peers, *value.shape)), axis, 0, 0, tiled=True
    )


def gather_directly(value, axis, dim):
    return in_order(sent_to_all(value, axis), dim)


def of_everyone(value, axis):
    everything = sent_to_all(value, axis)
    return jnp.sum(everything, axis=0)


def in_one(arrays, axis):
    ends = [0]
    for a in arrays:
        ends.append(ends[-1] + a.size)
    so_far = of_everyone(jnp.concatenate([a.ravel() for a in arrays]), axis)
    return tuple((so_far[b:e].reshape(a.shape) for a, b, e in zip(arrays, ends, ends[1:])))


def sent_together(arrays, axis, split_dim, concat_dim, along):
    both = jnp.concatenate(arrays, axis=along)
    whole, at, outs = (
        lax.all_to_all(both, axis, split_axis=split_dim, concat_axis=concat_dim, tiled=True),
        0,
        [],
    )
    for a in arrays:
        outs.append(lax.slice_in_dim(whole, at, at + a.shape[along], axis=along))
        at += a.shape[along]
    return tuple(outs)


def gathered_once(value, axis):
    leaves = jax.tree.leaves(value)
    order = sorted(range(len(leaves)), key=lambda k: -leaves[k].size)
    width = (1, *leaves[order[0]].shape)[-1]
    lines = [
        jnp.pad(leaves[k].reshape(-1), (0, -leaves[k].size % width)).reshape(-1, width)
        for k in order
    ]
    both, at, found = (lax.all_gather(jnp.concatenate(lines), axis), 0, {})
    for k, line in zip(order, lines):
        slab = both[:, at : at + len(line)].reshape(len(both), -1)
        found[k] = slab[:, : leaves[k].size].reshape(-1, *leaves[k].shape)
        at += len(line)
    numbers = iter(range(len(leaves)))
    return jax.tree.map(lambda _: found[next(numbers)], value)


def combined_by_axis(value, axes, combine):
    for axis in axes:
        pieces = gathered_once(
            jax.tree.map(
                lambda part, kind: part.astype(kind),
                value,
                (jnp.bfloat16, jnp.bfloat16, jnp.bfloat16),
            ),
            axis,
        )
        widened = [
            jax.tree.map(lambda part, own: part[k].astype(own.dtype), pieces, value)
            for k in range(lax.axis_size(axis))
        ]
        value = widened[0]
        for received in widened[1:]:
            value = combine(value, received)
    return value


def cut_along(value, dim, peers):
    dims = value.shape
    parts = value.reshape(*dims[:dim], peers, dims[dim] // peers, *dims[dim + 1 :])
    return jnp.moveaxis(parts, dim, 0)


def sum_at_owner(value, axis, dim):
    peers = lax.axis_size(axis)
    parts = lax.all_to_all(cut_along(value, dim, peers), axis, 0, 0, tiled=True)
    return jnp.sum(parts, axis=0)


def rotate(values, positions):
    half_dim = values.shape[-1] // 2
    inv_freq = 10000.0 ** (-jnp.arange(half_dim, dtype=jnp.float32) / half_dim)
    angles = positions.astype(jnp.float32)[..., None] * inv_freq
    cos_part = jnp.cos(angles)
    sin_part = jnp.sin(angles)
    lower = values[..., :half_dim]
    upper = values[..., half_dim:]
    return jnp.concatenate(
        [lower * cos_part - upper * sin_part, upper * cos_part + lower * sin_part], axis=-1
    )


def combine(earlier, later):
    max_one, sum_one, out_one = earlier
    max_two, sum_two, out_two = later
    new_max = jnp.maximum(max_one, max_two)
    weight_one = sum_one * jnp.exp(max_one - new_max)
    weight_two = sum_two * jnp.exp(max_two - new_max)
    merged = weight_one + weight_two
    safe_sum = jnp.where(merged > 0, merged, 1.0)
    result = (
        weight_one[..., None] * out_one.astype(jnp.float32)
        + weight_two[..., None] * out_two.astype(jnp.float32)
    ) / safe_sum[..., None]
    return (new_max, merged, result.astype(jnp.bfloat16))


def per_device(
    tokens,
    lengths,
    gain_attn,
    w_query_nope,
    w_query_rope,
    w_latent,
    w_rope_key,
    gain_latent,
    w_key_up,
    w_value_up,
    w_out,
    gain_mlp,
    w_up,
    w_down,
    cache_latent,
    cache_rope,
):
    kv_index = lax.axis_index(KV)
    tp_index = lax.axis_index("tp")
    seq_dev = cache_latent.shape[0]
    cache_dev = cache_latent.shape[1]
    heads_dev = w_key_up.shape[1] // NOPE
    block_cols = gather_directly(tokens, "tp", 1)
    batch_rows = block_cols.shape[0]
    widened = block_cols.astype(jnp.float32)
    square_piece = jnp.sum(widened * widened, axis=1)
    scaled = (widened * gain_attn).astype(jnp.bfloat16)
    part_nope = jnp.dot(scaled, w_query_nope, preferred_element_type=jnp.float32)
    part_rope = jnp.dot(scaled, w_query_rope, preferred_element_type=jnp.float32)
    own_rows = lax.dynamic_slice_in_dim(scaled, tp_index * seq_dev, seq_dev, 0)
    part_latent = jnp.dot(own_rows, w_latent, preferred_element_type=jnp.float32)
    part_key = jnp.dot(own_rows, w_rope_key, preferred_element_type=jnp.float32)
    square_sum, nope_sum, rope_sum, latent_sum, key_sum = in_one(
        (square_piece, part_nope, part_rope, part_latent, part_key), KV
    )
    inv_rms = lax.rsqrt(square_sum / D + EPS)
    q_nope = (nope_sum * inv_rms[:, None]).astype(jnp.bfloat16).reshape(batch_rows, heads_dev, NOPE)
    rope_raw = (rope_sum * inv_rms[:, None]).reshape(batch_rows, heads_dev, ROPE)
    q_rope = rotate(rope_raw, lengths[:, None]).astype(jnp.bfloat16)
    key_up = w_key_up.reshape(RANK, heads_dev, NOPE)
    q_latent = jnp.einsum(
        "bhn,rhn->bhr", q_nope, key_up, preferred_element_type=jnp.float32
    ).astype(jnp.bfloat16)
    latent_query, rope_query = sent_together((q_latent, q_rope), "tp", 0, 1, 2)
    own_inv = lax.dynamic_slice_in_dim(inv_rms, tp_index * seq_dev, seq_dev, 0)
    own_len = lax.dynamic_slice_in_dim(lengths, tp_index * seq_dev, seq_dev, 0)
    raw_latent = latent_sum * own_inv[:, None]
    latent_new = (
        raw_latent
        * lax.rsqrt(jnp.mean(raw_latent * raw_latent, axis=1, keepdims=True) + EPS)
        * gain_latent
    ).astype(jnp.bfloat16)
    key_new = rotate(key_sum * own_inv[:, None], own_len).astype(jnp.bfloat16)
    score_scale = (NOPE + ROPE) ** (-0.5)
    positions = kv_index * cache_dev + jnp.arange(cache_dev, dtype=jnp.int32)
    rotated = rotate(cache_rope.astype(jnp.float32), positions).astype(jnp.bfloat16)
    scores = (
        jnp.einsum("shr,spr->shp", latent_query, cache_latent, preferred_element_type=jnp.float32)
        + jnp.einsum("shk,spk->shp", rope_query, rotated, preferred_element_type=jnp.float32)
    ) * score_scale
    live_mask = positions[None, None, :] < own_len[:, None, None]
    block_max = jnp.max(jnp.where(live_mask, scores, -1e30), axis=2)
    exponent = jnp.where(live_mask, jnp.exp(scores - block_max[..., None]), 0.0)
    block_sum = jnp.sum(exponent, axis=2)
    weighted = jnp.einsum(
        "shp,spr->shr",
        exponent.astype(jnp.bfloat16),
        cache_latent,
        preferred_element_type=jnp.float32,
    )
    block_out = (weighted / jnp.where(block_sum > 0, block_sum, 1.0)[..., None]).astype(
        jnp.bfloat16
    )
    block_max, block_sum, block_out = combined_by_axis(
        (block_max, block_sum, block_out), KV, combine
    )
    own_score = (
        jnp.einsum("shr,sr->sh", latent_query, latent_new, preferred_element_type=jnp.float32)
        + jnp.einsum("shk,sk->sh", rope_query, key_new, preferred_element_type=jnp.float32)
    ) * score_scale
    new_max = jnp.maximum(block_max, own_score)
    carried = block_sum * jnp.exp(block_max - new_max)
    own_weight = jnp.exp(own_score - new_max)
    o_latent = (
        (
            carried[..., None] * block_out.astype(jnp.float32)
            + own_weight[..., None] * latent_new.astype(jnp.float32)[:, None, :]
        )
        / (carried + own_weight)[..., None]
    ).astype(jnp.bfloat16)
    head_latent = lax.all_to_all(o_latent, "tp", split_axis=1, concat_axis=0, tiled=True)
    value_up = w_value_up.reshape(RANK, heads_dev, VD)
    head_out = (
        jnp.einsum("bhr,rhv->bhv", head_latent, value_up, preferred_element_type=jnp.float32)
        .astype(jnp.bfloat16)
        .reshape(batch_rows, heads_dev * VD)
    )
    attn_part = jnp.dot(head_out, w_out, preferred_element_type=jnp.float32)
    attn_sum = of_everyone(attn_part, "tp")
    resid = (widened + attn_sum).astype(jnp.bfloat16)
    resid_wide = resid.astype(jnp.float32)
    square_two = jnp.sum(resid_wide * resid_wide, axis=1)
    scaled2 = (resid_wide * gain_mlp).astype(jnp.bfloat16)
    up_part = jnp.dot(scaled2, w_up, preferred_element_type=jnp.float32)
    spread_squares = jnp.broadcast_to(square_two[:, None], (batch_rows, lax.axis_size(KV)))
    up_share, square_cols = (sum_at_owner(up_part, KV, 1), sum_at_owner(spread_squares, KV, 1))
    square_all = square_cols[:, 0]
    active_share = jnp.square(jnp.maximum(up_share, 0.0)).astype(jnp.bfloat16)
    activated = gather_directly(active_share, KV, 1)
    inv_rms2 = lax.rsqrt(square_all / D + EPS)
    down_part = jnp.dot(activated, w_down, preferred_element_type=jnp.float32)
    down_sum = sum_at_owner(down_part, "tp", 1)
    out_cols = down_sum.shape[1]
    resid_cols = lax.dynamic_slice_in_dim(resid_wide, tp_index * out_cols, out_cols, 1)
    return (resid_cols + (inv_rms2 * inv_rms2)[:, None] * down_sum).astype(jnp.bfloat16)


def solution(mesh):
    split = Mesh(mesh.devices.reshape(4, 4, mesh.shape["tp"]), ("kv_0", "kv_1", "tp"))
    in_specs = (
        P(None, KV_TP),
        P(),
        P(KV),
        P(KV, "tp"),
        P(KV, "tp"),
        P(KV, None),
        P(KV, None),
        P(),
        P(None, "tp"),
        P(None, "tp"),
        P("tp", KV),
        P(KV),
        P(KV, "tp"),
        P("tp", KV),
        P("tp", KV, None),
        P("tp", KV, None),
    )
    out_specs = P(None, KV_TP)
    return jax.shard_map(
        per_device, mesh=split, in_specs=in_specs, out_specs=out_specs, check_vma=False
    )
```

profile of v0, /device:TPU:1, one launch (start us, length us, event | category | flops | bytes accessed | tf_op | source)
XLA Modules:
  0.0 297.0 jit_solution(5420267243332962274)
XLA Ops:
  1.6 16.7 %all-to-all-start = ((bf16[32,2,256]{2,1,0:T(2,128)(2,1)}), bf16[32,2,256]{2,1,0:T(2,128)(2,1)S(1)}, u32[]{:S(2)}, u32[]{:S(2)}) async-start(bf16[32,2,256]{2,1,0:T(2,128)(2,1)} %reshape.1051), calls=%async_computation | async-start | bytes 65536 | tf_op jit(solution)/shard_map/all_to_all | solution.py:27
  18.3 1.3 fusion.113
  22.5 7.9 %all-to-all-done = bf16[32,2,256]{2,1,0:T(2,128)(2,1)S(1)} async-done(((bf16[32,2,256]{2,1,0:T(2,128)(2,1)}), bf16[32,2,256]{2,1,0:T(2,128)(2,1)S(1)}, u32[]{:S(2)}, u32[]{:S(2)}) %all-to-all-start) | async-done | bytes 32800 | tf_op jit(solution)/shard_map/all_to_all | solution.py:27
  35.7 1.4 broadcast_in_dim.40
  37.1 6.8 %all-to-all-start.1 = ((f32[16,1,13504]{2,1,0:T(1,128)}), f32[16,1,13504]{2,1,0:T(1,128)S(1)}, u32[]{:S(2)}, u32[]{:S(2)}) async-start(f32[16,1,13504]{2,1,0:T(1,128)} %broadcast_in_dim.40), calls=%async_computation.1 | async-start | bytes 1736704 | tf_op jit(solution)/shard_map/all_to_all | solution.py:27
  43.9 1.4 broadcast_compare_fusion
  47.3 10.2 %all-to-all-done.1 = f32[16,1,13504]{2,1,0:T(1,128)S(1)} async-done(((f32[16,1,13504]{2,1,0:T(1,128)}), f32[16,1,13504]{2,1,0:T(1,128)S(1)}, u32[]{:S(2)}, u32[]{:S(2)}) %all-to-all-start.1) | async-done | bytes 864288 | tf_op jit(solution)/shard_map/all_to_all | solution.py:27
  62.7 6.5 %all-to-all-start.2 = ((bf16[32,2,576]{2,1,0:T(2,128)(2,1)}), bf16[32,2,576]{2,1,0:T(2,128)(2,1)S(1)}, u32[]{:S(2)}, u32[]{:S(2)}) async-start(bf16[32,2,576]{2,1,0:T(2,128)(2,1)} %reshape.1053), calls=%async_computation.2 | async-start | bytes 163840 | tf_op jit(solution)/shard_map/all_to_all | solution.py:52
  69.9 13.1 %all-to-all-done.2 = bf16[32,2,576]{2,1,0:T(2,128)(2,1)S(1)} async-done(((bf16[32,2,576]{2,1,0:T(2,128)(2,1)}), bf16[32,2,576]{2,1,0:T(2,128)(2,1)S(1)}, u32[]{:S(2)}, u32[]{:S(2)}) %all-to-all-start.2) | async-done | bytes 73760 | tf_op jit(solution)/shard_map/all_to_all | solution.py:52
  85.6 9.5 %all-gather.2 = bf16[4,66,512]{2,1,0:T(8,128)(2,1)S(1)} all-gather(bf16[1,66,512]{2,1,0:T(8,128)(2,1)S(1)} %maximum_bitcast_fusion), channel_id=2, replica_groups=mesh['kv_0'=4,'kv_1'=4,'tp'=32] {'kv_0'}, dimensions={0}, use_global_device_ids=true | all-gather | bytes 337920 | tf_op jit(solution)/shard_map/all_gather | solution.py:70
  95.5 10.0 %all-gather.3 = bf16[4,66,512]{2,1,0:T(8,128)(2,1)S(1)} all-gather(bf16[1,66,512]{2,1,0:T(8,128)(2,1)S(1)} %maximum_bitcast_fusion.1), channel_id=3, replica_groups=mesh['kv_0'=4,'kv_1'=4,'tp'=32] {'kv_1'}, dimensions={0}, use_global_device_ids=true | all-gather | bytes 337920 | tf_op jit(solution)/shard_map/all_gather | solution.py:70
  106.8 22.7 %all_to_all.69 = bf16[2,32,512]{2,0,1:T(2,128)(2,1)S(1)} all-to-all(bf16[2,32,512]{2,0,1:T(2,128)(2,1)S(1)} %copy.231), channel_id=1, replica_groups=mesh['kv_0'=4,'kv_1'=4,'tp'=32] {'tp'}, dimensions={1} | all-to-all | bytes 131072 | tf_op jit(solution)/shard_map/all_to_all | solution.py:230
  129.8 1.5 broadcast_in_dim.45
  131.4 6.1 %all-to-all-start.4 = ((f32[32,64,256]{2,1,0:T(8,128)}), f32[32,64,256]{2,1,0:T(8,128)}, u32[]{:S(2)}, u32[]{:S(2)}) async-start(f32[32,64,256]{2,1,0:T(8,128)} %broadcast_in_dim.45), calls=%async_computation.4 | async-start | bytes 4194304 | tf_op jit(solution)/shard_map/all_to_all | solution.py:27
  137.8 98.7 %all-to-all-done.4 = f32[32,64,256]{2,1,0:T(8,128)} async-done(((f32[32,64,256]{2,1,0:T(8,128)}), f32[32,64,256]{2,1,0:T(8,128)}, u32[]{:S(2)}, u32[]{:S(2)}) %all-to-all-start.4) | async-done | bytes 2097184 | tf_op jit(solution)/shard_map/all_to_all | solution.py:27
  236.5 1.7 reduce_sum.87
  239.4 3.5 %all-to-all-start.6 = ((f32[16,1,2048]{2,1,0:T(1,128)}), f32[16,1,2048]{2,1,0:T(1,128)S(1)}, u32[]{:S(2)}, u32[]{:S(2)}) async-start(f32[16,1,2048]{2,1,0:T(1,128)} %reshape.1055), calls=%async_computation.6 | async-start | bytes 262144 | tf_op jit(solution)/shard_map/all_to_all | solution.py:107
  243.1 6.6 %all-to-all-done.6 = f32[16,1,2048]{2,1,0:T(1,128)S(1)} async-done(((f32[16,1,2048]{2,1,0:T(1,128)}), f32[16,1,2048]{2,1,0:T(1,128)S(1)}, u32[]{:S(2)}, u32[]{:S(2)}) %all-to-all-start.6) | async-done | bytes 131104 | tf_op jit(solution)/shard_map/all_to_all | solution.py:107
  252.2 3.5 %all-to-all-start.7 = ((bf16[16,2,1024]{2,1,0:T(2,128)(2,1)}), bf16[16,2,1024]{2,1,0:T(2,128)(2,1)S(1)}, u32[]{:S(2)}, u32[]{:S(2)}) async-start(bf16[16,2,1024]{2,1,0:T(2,128)(2,1)} %reshape.1057), calls=%async_computation.7 | async-start | bytes 131072 | tf_op jit(solution)/shard_map/all_to_all | solution.py:27
  255.7 6.4 %all-to-all-done.7 = bf16[16,2,1024]{2,1,0:T(2,128)(2,1)S(1)} async-done(((bf16[16,2,1024]{2,1,0:T(2,128)(2,1)}), bf16[16,2,1024]{2,1,0:T(2,128)(2,1)S(1)}, u32[]{:S(2)}, u32[]{:S(2)}) %all-to-all-start.7) | async-done | bytes 65568 | tf_op jit(solution)/shard_map/all_to_all | solution.py:27
  262.7 3.4 %all-to-all-start.5 = ((f32[16,64,1]{1,2,0:T(1,128)}), f32[16,64,1]{1,2,0:T(1,128)S(1)}, u32[]{:S(2)}, u32[]{:S(2)}) async-start(f32[16,64,1]{1,2,0:T(1,128)} %transpose.85), calls=%async_computation.5 | async-start | bytes 16384 | tf_op jit(solution)/shard_map/all_to_all | solution.py:107
  267.4 5.2 %all-to-all-done.5 = f32[16,64,1]{1,2,0:T(1,128)S(1)} async-done(((f32[16,64,1]{1,2,0:T(1,128)}), f32[16,64,1]{1,2,0:T(1,128)S(1)}, u32[]{:S(2)}, u32[]{:S(2)}) %all-to-all-start.5) | async-done | bytes 4128 | tf_op jit(solution)/shard_map/all_to_all | solution.py:107
  272.6 9.9 %all-to-all-start.8 = ((f32[32,1,512]{2,1,0:T(1,128)}), f32[32,1,512]{2,1,0:T(1,128)S(1)}, u32[]{:S(2)}, u32[]{:S(2)}) async-start(f32[32,1,512]{2,1,0:T(1,128)} %reshape.1059), calls=%async_computation.8 | async-start | bytes 131072 | tf_op jit(solution)/shard_map/all_to_all | solution.py:107
  282.5 13.0 %all-to-all-done.8 = f32[32,1,512]{2,1,0:T(1,128)S(1)} async-done(((f32[32,1,512]{2,1,0:T(1,128)}), f32[32,1,512]{2,1,0:T(1,128)S(1)}, u32[]{:S(2)}, u32[]{:S(2)}) %all-to-all-start.8) | async-done | bytes 65568 | tf_op jit(solution)/shard_map/all_to_all | solution.py:107
  (151 shorter events, 29.3 us)
Async XLA Ops:
  0.0 83.6 %copy-start = (bf16[2,1024,512]{2,1,0:T(8,128)(2,1)S(1)}, bf16[2,1024,512]{2,1,0:T(8,128)(2,1)}, u32[]{:S(2)}) copy-start(bf16[2,1024,512]{2,1,0:T(8,128)(2,1)} %param.30) | copy-start | bytes 6291460
  1.6 28.8 %all-to-all-start = ((bf16[32,2,256]{2,1,0:T(2,128)(2,1)}), bf16[32,2,256]{2,1,0:T(2,128)(2,1)S(1)}, u32[]{:S(2)}, u32[]{:S(2)}) async-start(bf16[32,2,256]{2,1,0:T(2,128)(2,1)} %reshape.1051), calls=%async_computation | async-start | bytes 65536 | tf_op jit(solution)/shard_map/all_to_all | solution.py:27
  37.1 20.4 %all-to-all-start.1 = ((f32[16,1,13504]{2,1,0:T(1,128)}), f32[16,1,13504]{2,1,0:T(1,128)S(1)}, u32[]{:S(2)}, u32[]{:S(2)}) async-start(f32[16,1,13504]{2,1,0:T(1,128)} %broadcast_in_dim.40), calls=%async_computation.1 | async-start | bytes 1736704 | tf_op jit(solution)/shard_map/all_to_all | solution.py:27
  43.9 1.4 copy-start.8
  47.2 22.4 %copy-start.9 = (f32[32]{0:T(128)S(1)}, f32[32]{0:T(128)}, u32[]{:S(2)}) copy-start(f32[32]{0:T(128)} %copy-done.8) | copy-start | bytes 388
  47.3 22.4 %copy-start.11 = (f32[2]{0:T(128)S(1)}, f32[2]{0:T(128)}, u32[]{:S(2)}) copy-start(f32[2]{0:T(128)} %get-tuple-element.28) | copy-start | bytes 28
  47.3 22.6 %copy-start.10 = (f32[512]{0:T(512)S(1)}, f32[512]{0:T(512)}, u32[]{:S(2)}) copy-start(f32[512]{0:T(512)} %param.23) | copy-start | bytes 6148
  59.5 24.8 %copy-start.1 = (bf16[2,1024,32]{1,2,0:T(8,128)(2,1)S(1)}, bf16[2,1024,32]{1,2,0:T(8,128)(2,1)}, u32[]{:S(2)}) copy-start(bf16[2,1024,32]{1,2,0:T(8,128)(2,1)} %get-tuple-element.41) | copy-start | bytes 393220
  59.5 24.8 %copy-start.2 = (bf16[2,1024,32]{1,2,0:T(8,128)(2,1)S(1)}, bf16[2,1024,32]{1,2,0:T(8,128)(2,1)}, u32[]{:S(2)}) copy-start(bf16[2,1024,32]{1,2,0:T(8,128)(2,1)} %get-tuple-element.42) | copy-start | bytes 393220
  59.6 24.8 %copy-start.6 = (pred[2,1024]{1,0:T(4,128)(4,1)S(1)}, pred[2,1024]{1,0:T(4,128)(4,1)}, u32[]{:S(2)}) copy-start(pred[2,1024]{1,0:T(4,128)(4,1)} %broadcast_compare_fusion) | copy-start | bytes 6148
  62.7 20.3 %all-to-all-start.2 = ((bf16[32,2,576]{2,1,0:T(2,128)(2,1)}), bf16[32,2,576]{2,1,0:T(2,128)(2,1)S(1)}, u32[]{:S(2)}, u32[]{:S(2)}) async-start(bf16[32,2,576]{2,1,0:T(2,128)(2,1)} %reshape.1053), calls=%async_computation.2 | async-start | bytes 163840 | tf_op jit(solution)/shard_map/all_to_all | solution.py:52
  85.4 44.2 %copy-start.5 = (bf16[512,128]{1,0:T(8,128)(2,1)S(1)}, bf16[512,128]{1,0:T(8,128)(2,1)}, u32[]{:S(2)}) copy-start(bf16[512,128]{1,0:T(8,128)(2,1)} %param.25) | copy-start | bytes 393220
  85.4 44.2 %copy-start.7 = (bf16[128,256]{1,0:T(8,128)(2,1)S(1)}, bf16[128,256]{1,0:T(8,128)(2,1)}, u32[]{:S(2)}) copy-start(bf16[128,256]{1,0:T(8,128)(2,1)} %param.26) | copy-start | bytes 196612
  131.4 6.1 %copy-start.3 = (bf16[256,512]{1,0:T(8,128)(2,1)S(1)}, bf16[256,512]{1,0:T(8,128)(2,1)}, u32[]{:S(2)}) copy-start(bf16[256,512]{1,0:T(8,128)(2,1)} %param.28) | copy-start | bytes 786436
  131.4 6.3 %copy-start.12 = (f32[256]{0:T(256)S(1)}, f32[256]{0:T(256)}, u32[]{:S(2)}) copy-start(f32[256]{0:T(256)} %param.27) | copy-start | bytes 3076
  131.4 105.1 %all-to-all-start.4 = ((f32[32,64,256]{2,1,0:T(8,128)}), f32[32,64,256]{2,1,0:T(8,128)}, u32[]{:S(2)}, u32[]{:S(2)}) async-start(f32[32,64,256]{2,1,0:T(8,128)} %broadcast_in_dim.45), calls=%async_computation.4 | async-start | bytes 4194304 | tf_op jit(solution)/shard_map/all_to_all | solution.py:27
  137.5 105.4 %copy-start.4 = (bf16[512,256]{1,0:T(8,128)(2,1)S(1)}, bf16[512,256]{1,0:T(8,128)(2,1)}, u32[]{:S(2)}) copy-start(bf16[512,256]{1,0:T(8,128)(2,1)} %param.29) | copy-start | bytes 786436
  239.4 10.3 %all-to-all-start.6 = ((f32[16,1,2048]{2,1,0:T(1,128)}), f32[16,1,2048]{2,1,0:T(1,128)S(1)}, u32[]{:S(2)}, u32[]{:S(2)}) async-start(f32[16,1,2048]{2,1,0:T(1,128)} %reshape.1055), calls=%async_computation.6 | async-start | bytes 262144 | tf_op jit(solution)/shard_map/all_to_all | solution.py:107
  252.2 10.0 %all-to-all-start.7 = ((bf16[16,2,1024]{2,1,0:T(2,128)(2,1)}), bf16[16,2,1024]{2,1,0:T(2,128)(2,1)S(1)}, u32[]{:S(2)}, u32[]{:S(2)}) async-start(bf16[16,2,1024]{2,1,0:T(2,128)(2,1)} %reshape.1057), calls=%async_computation.7 | async-start | bytes 131072 | tf_op jit(solution)/shard_map/all_to_all | solution.py:27
  262.7 9.8 %all-to-all-start.5 = ((f32[16,64,1]{1,2,0:T(1,128)}), f32[16,64,1]{1,2,0:T(1,128)S(1)}, u32[]{:S(2)}, u32[]{:S(2)}) async-start(f32[16,64,1]{1,2,0:T(1,128)} %transpose.85), calls=%async_computation.5 | async-start | bytes 16384 | tf_op jit(solution)/shard_map/all_to_all | solution.py:107
  272.6 22.9 %all-to-all-start.8 = ((f32[32,1,512]{2,1,0:T(1,128)}), f32[32,1,512]{2,1,0:T(1,128)S(1)}, u32[]{:S(2)}, u32[]{:S(2)}) async-start(f32[32,1,512]{2,1,0:T(1,128)} %reshape.1059), calls=%async_computation.8 | async-start | bytes 131072 | tf_op jit(solution)/shard_map/all_to_all | solution.py:107
where the time goes:
time: 298 us; the launch traced here: 297 us
  waiting for transfers between devices  161 us (54%)
  starting transfers between devices  56.5 us (19%)
  blocking collectives  42.2 us (14%)
  other arithmetic  16.5 us (6%)
  local copies, waits for them, and re-layouts  12.3 us (4%)
  matrix products  7.83 us (3%)
    all_to_all x4, waiting for transfers between devices, sent_to_all(): lax.all_to_all(jnp.broadcast_to(value[None], (peers, *value.shape)), axis...  123 us
    all_to_all x4, starting transfers between devices, sent_to_all(): lax.all_to_all(jnp.broadcast_to(value[None], (peers, *value.shape)), axis...  33.1 us
    all_to_all x3, waiting for transfers between devices, sum_at_owner(): parts = lax.all_to_all(cut_along(value, dim, peers), axis, 0, 0, tiled=True)  24.8 us
    all_to_all x1, blocking collectives, per_device(): lax.all_to_all(o_latent, 'tp', split_axis=1, concat_axis=0, tiled=True)  22.7 us
    all_gather x2, blocking collectives, gathered_once(): both, at, found = (lax.all_gather(jnp.concatenate(lines), axis), 0, {})  19.5 us
    all_to_all x3, starting transfers between devices, sum_at_owner(): parts = lax.all_to_all(cut_along(value, dim, peers), axis, 0, 0, tiled=True)  16.9 us
    all_to_all x1, waiting for transfers between devices, sent_together(): lax.all_to_all(both, axis, split_axis=split_dim, concat_axis=concat_dim,...  13.1 us
    all_to_all x1, starting transfers between devices, sent_together(): lax.all_to_all(both, axis, split_axis=split_dim, concat_axis=concat_dim,...  6.55 us
  transfers between devices with their start and end apart: 8, of which 8 were waited for; matrix products, arithmetic and copies ran while one was open for 3% of the time, Pallas kernels for 0%

commit v1 on v0

v1 whole, which is shorter than its diff:
```python
import jax
import jax.numpy as jnp
from jax import lax
from jax.sharding import Mesh
from jax.sharding import PartitionSpec as P

D = 4096
NOPE = 128
ROPE = 64
VD = 128
RANK = 512
KV = ("kv_0", "kv_1")
KV_TP = ("kv_0", "kv_1", "tp")
EPS = 1e-06
BF = jnp.bfloat16
F32 = jnp.float32


def exchange(parts, axis):
    return lax.all_to_all(parts, axis, 0, 0, tiled=True)


def to_all(value, axis):
    peers = lax.axis_size(axis)
    return exchange(jnp.broadcast_to(value[None], (peers, *value.shape)), axis)


def split3(x):
    hi = lax.reduce_precision(x, 8, 7)
    rest = x - hi
    mid = lax.reduce_precision(rest, 8, 7)
    low = rest - mid
    return hi.astype(BF), mid.astype(BF), low.astype(BF)


def join3(hi, mid, low):
    return hi.astype(F32) + (mid.astype(F32) + low.astype(F32))


def rotate(values, positions):
    half_dim = values.shape[-1] // 2
    inv_freq = 10000.0 ** (-jnp.arange(half_dim, dtype=F32) / half_dim)
    angles = positions.astype(F32)[..., None] * inv_freq
    cos_part = jnp.cos(angles)
    sin_part = jnp.sin(angles)
    lower = values[..., :half_dim]
    upper = values[..., half_dim:]
    return jnp.concatenate(
        [lower * cos_part - upper * sin_part, upper * cos_part + lower * sin_part], axis=-1
    )


def per_device(
    tokens,
    lengths,
    gain_attn,
    w_query_nope,
    w_query_rope,
    w_latent,
    w_rope_key,
    gain_latent,
    w_key_up,
    w_value_up,
    w_out,
    gain_mlp,
    w_up,
    w_down,
    cache_latent,
    cache_rope,
):
    kv_index = lax.axis_index(KV)
    tp_index = lax.axis_index("tp")
    n_kv = lax.axis_size(KV)
    n_tp = lax.axis_size("tp")
    seq_dev, cache_dev = cache_latent.shape[:2]
    batch = tokens.shape[0]

    block_t = to_all(tokens.T, "tp").reshape(-1, batch)
    wide_t = block_t.astype(F32)
    square_piece = jnp.sum(wide_t * wide_t, axis=0)
    scaled_t = (wide_t * gain_attn[:, None]).astype(BF)
    dims = (((0,), (0,)), ((), ()))
    part_nope = lax.dot_general(scaled_t, w_query_nope, dims, preferred_element_type=F32)
    part_rope = lax.dot_general(scaled_t, w_query_rope, dims, preferred_element_type=F32)
    own_rows = lax.dynamic_slice_in_dim(scaled_t, tp_index * seq_dev, seq_dev, 1)
    part_latent = lax.dot_general(own_rows, w_latent, dims, preferred_element_type=F32)
    part_key = lax.dot_general(own_rows, w_rope_key, dims, preferred_element_type=F32)
    lane = 128
    pieces = [part_nope, part_rope, part_latent, part_key, square_piece]
    flat = [
        jnp.pad(p.reshape(-1), (0, -p.size % lane)).reshape(-1, lane).astype(BF) for p in pieces
    ]
    rows = [f.shape[0] for f in flat]
    packed = jnp.concatenate(flat, axis=0)
    packed = jnp.pad(packed, ((0, -packed.shape[0] % 16), (0, 0)))
    total = jnp.sum(to_all(packed, KV).astype(F32), axis=0)
    at = 0
    sums = []
    for p, r in zip(pieces, rows):
        sums.append(total[at : at + r].reshape(-1)[: p.size].reshape(p.shape))
        at += r
    nope_sum, rope_sum, latent_sum, key_sum, square_sum = sums
    inv_rms = lax.rsqrt(square_sum / D + EPS)
    q_nope = (nope_sum * inv_rms[:, None]).astype(BF)
    q_rope = rotate(rope_sum * inv_rms[:, None], lengths).astype(BF)
    q_latent = lax.dot_general(
        q_nope, w_key_up, (((1,), (1,)), ((), ())), preferred_element_type=F32
    ).astype(BF)
    query = jnp.concatenate([q_latent, q_rope], axis=1)
    query = exchange(query.reshape(n_tp, seq_dev, RANK + ROPE), "tp")
    latent_query = jnp.swapaxes(query[:, :, :RANK], 0, 1)
    rope_query = jnp.swapaxes(query[:, :, RANK:], 0, 1)

    own_inv = lax.dynamic_slice_in_dim(inv_rms, tp_index * seq_dev, seq_dev, 0)
    own_len = lax.dynamic_slice_in_dim(lengths, tp_index * seq_dev, seq_dev, 0)
    raw_latent = latent_sum * own_inv[:, None]
    latent_new = (
        raw_latent
        * lax.rsqrt(jnp.mean(raw_latent * raw_latent, axis=1, keepdims=True) + EPS)
        * gain_latent
    ).astype(BF)
    key_new = rotate(key_sum * own_inv[:, None], own_len).astype(BF)

    score_scale = (NOPE + ROPE) ** (-0.5)
    positions = kv_index * cache_dev + jnp.arange(cache_dev, dtype=jnp.int32)
    rotated = rotate(cache_rope.astype(F32), positions).astype(BF)
    scores = (
        jnp.einsum("shr,spr->shp", latent_query, cache_latent, preferred_element_type=F32)
        + jnp.einsum("shk,spk->shp", rope_query, rotated, preferred_element_type=F32)
    ) * score_scale
    own_score = (
        jnp.einsum("shr,sr->sh", latent_query, latent_new, preferred_element_type=F32)
        + jnp.einsum("shk,sk->sh", rope_query, key_new, preferred_element_type=F32)
    ) * score_scale
    first = kv_index == 0
    own_score = jnp.where(first, own_score, -1e30)
    live = positions[None, None, :] < own_len[:, None, None]
    peak = jnp.maximum(jnp.max(jnp.where(live, scores, -1e30), axis=2), own_score)
    expo = jnp.where(live, jnp.exp(scores - peak[..., None]), 0.0)
    own_weight = jnp.where(first, jnp.exp(own_score - peak), 0.0)
    mass = jnp.sum(expo, axis=2) + own_weight
    weighted = jnp.einsum(
        "shp,spr->shr", expo.astype(BF), cache_latent, preferred_element_type=F32
    )
    weighted = weighted + own_weight[..., None] * latent_new.astype(F32)[:, None, :]
    block_out = (weighted / jnp.where(mass > 0, mass, 1.0)[..., None]).astype(BF)

    stats = jnp.stack([*split3(peak), *split3(mass)], axis=-1)
    stats = jnp.pad(stats, ((0, 0), (0, 0), (0, lane - stats.shape[-1])))
    sent = jnp.concatenate([block_out, stats], axis=-1)
    got = exchange(jnp.swapaxes(sent, 0, 1), "tp").reshape(batch, RANK + lane)
    head_part = jnp.dot(got[:, :RANK], w_value_up, preferred_element_type=F32).astype(BF)
    both = jnp.concatenate([head_part, got[:, RANK:]], axis=1)
    blocks = to_all(both, KV)
    peaks = join3(blocks[:, :, VD], blocks[:, :, VD + 1], blocks[:, :, VD + 2])
    masses = join3(blocks[:, :, VD + 3], blocks[:, :, VD + 4], blocks[:, :, VD + 5])
    top = jnp.max(peaks, axis=0)
    weight = masses * jnp.exp(peaks - top)
    weight = weight / jnp.sum(weight, axis=0)
    head_out = jnp.sum(weight[..., None] * blocks[:, :, :VD].astype(F32), axis=0).astype(BF)

    attn_part = jnp.dot(head_out, w_out, preferred_element_type=F32).astype(BF)
    width = attn_part.shape[1]
    attn_rows = jnp.sum(
        exchange(attn_part.reshape(n_tp, seq_dev, width), "tp").astype(F32), axis=0
    )
    own_cols = lax.dynamic_slice_in_dim(block_t, tp_index * seq_dev, seq_dev, 1)
    resid_rows = (own_cols.T.astype(F32) + attn_rows).astype(BF)
    resid = to_all(resid_rows, "tp").reshape(batch, width)
    resid_wide = resid.astype(F32)
    square_two = jnp.sum(resid_wide * resid_wide, axis=1, keepdims=True)
    scaled2 = (resid_wide * gain_mlp).astype(BF)
    up_part = jnp.dot(scaled2, w_up, preferred_element_type=F32)
    units = up_part.shape[1]
    up_sent = jnp.concatenate(
        [up_part, jnp.broadcast_to(square_two, (batch, lane))], axis=1
    ).astype(BF)
    up_got = exchange(up_sent.reshape(n_kv, batch // n_kv, units + lane), KV)
    up_all = jnp.sum(up_got.astype(F32), axis=0)
    inv_rms2 = lax.rsqrt(up_all[:, units:units + 1] / D + EPS)
    active = jnp.square(jnp.maximum(up_all[:, :units], 0.0) * inv_rms2).astype(BF)
    activated = to_all(active, KV).reshape(batch, units)
    down_t = lax.dot_general(
        w_down, activated, (((0,), (1,)), ((), ())), preferred_element_type=F32
    ).astype(BF)
    out_cols = width // n_tp
    down_sum = jnp.sum(
        exchange(down_t.reshape(n_tp, out_cols, batch), "tp").astype(F32), axis=0
    )
    resid_cols = lax.dynamic_slice_in_dim(resid_wide, tp_index * out_cols, out_cols, 1)
    return (resid_cols + down_sum.T).astype(BF)


def solution(mesh):
    split = Mesh(mesh.devices.reshape(4, 4, mesh.shape["tp"]), ("kv_0", "kv_1", "tp"))
    in_specs = (
        P(None, KV_TP),
        P(),
        P(KV),
        P(KV, "tp"),
        P(KV, "tp"),
        P(KV, None),
        P(KV, None),
        P(),
        P(None, "tp"),
        P(None, "tp"),
        P("tp", KV),
        P(KV),
        P(KV, "tp"),
        P("tp", KV),
        P("tp", KV, None),
        P("tp", KV, None),
    )
    out_specs = P(None, KV_TP)
    return jax.shard_map(
        per_device, mesh=split, in_specs=in_specs, out_specs=out_specs, check_vma=False
    )
```

time: 298 us -> 196 us (0.66)
  waiting for transfers between devices: 161 us -> 54 us
  blocking collectives: 42.2 us -> 65.8 us
  starting transfers between devices: 56.5 us -> 42.6 us
  other arithmetic: 16.5 us -> 11.4 us
    all_to_all x8 -> x5, waiting for transfers between devices: 161 us -> 54 us  [exchange(): return lax.all_to_all(parts, axis, 0, 0, tiled=True)]
    all_to_all x1 -> x5, blocking collectives: 22.7 us -> 65.8 us  [exchange(): return lax.all_to_all(parts, axis, 0, 0, tiled=True)]
    all_gather x2 -> x0, blocking collectives: 19.5 us -> none  [gathered_once(): both, at, found = (lax.all_gather(jnp.concatenate(lines), axis), 0, {})]
    all_to_all x8 -> x5, starting transfers between devices: 56.5 us -> 42.6 us  [exchange(): return lax.all_to_all(parts, axis, 0, 0, tiled=True)]
    unnamed x45 -> x25, local copies, waits for them, and re-layouts: 5.45 us -> 6.43 us
    dot_general x11 -> x12, matrix products: 7 us -> 6.94 us  [the longest x1 1.2 us: per_device(): lax.dot_general(own_rows, w_latent, dims, preferred_element_type=F32)]
  transfers between devices with their start and end apart: 8 -> 5, of which waited for: 8 -> 5; matrix products, arithmetic and copies ran while one was open for 3% -> 3% of each run, Pallas kernels for 0% -> 0%
where the time goes in v1:
time: 196 us; the launch traced here: 195 us
  blocking collectives  65.8 us (34%)
  waiting for transfers between devices  54 us (28%)
  starting transfers between devices  42.6 us (22%)
  local copies, waits for them, and re-layouts  12.7 us (6%)
  other arithmetic  11.4 us (6%)
  matrix products  7.78 us (4%)
    all_to_all x5, blocking collectives, exchange(): return lax.all_to_all(parts, axis, 0, 0, tiled=True)  65.8 us
    all_to_all x5, waiting for transfers between devices, exchange(): return lax.all_to_all(parts, axis, 0, 0, tiled=True)  54 us
    all_to_all x5, starting transfers between devices, exchange(): return lax.all_to_all(parts, axis, 0, 0, tiled=True)  42.6 us
    unnamed x25, local copies, waits for them, and re-layouts  6.43 us
  transfers between devices with their start and end apart: 5, of which 5 were waited for; matrix products, arithmetic and copies ran while one was open for 3% of the time, Pallas kernels for 0%

profile of v1, /device:TPU:1, one launch (start us, length us, event | category | flops | bytes accessed | tf_op | source)
XLA Modules:
  0.0 194.6 jit_solution(5960953564548982949)
XLA Ops:
  1.6 16.7 %all-to-all-start = ((bf16[32,2,256]{2,1,0:T(2,128)(2,1)}), bf16[32,2,256]{2,1,0:T(2,128)(2,1)S(1)}, u32[]{:S(2)}, u32[]{:S(2)}) async-start(bf16[32,2,256]{2,1,0:T(2,128)(2,1)} %reshape.288), calls=%async_computation | async-start | bytes 65536 | tf_op jit(solution)/shard_map/all_to_all | solution.py:20
  18.4 1.2 multiply_cosine_fusion
  20.3 1.2 convert_element_type.223
  22.5 7.9 %all-to-all-done = bf16[32,2,256]{2,1,0:T(2,128)(2,1)S(1)} async-done(((bf16[32,2,256]{2,1,0:T(2,128)(2,1)}), bf16[32,2,256]{2,1,0:T(2,128)(2,1)S(1)}, u32[]{:S(2)}, u32[]{:S(2)}) %all-to-all-start) | async-done | bytes 32800 | tf_op jit(solution)/shard_map/all_to_all | solution.py:20
  32.4 1.2 convolution_convert_fusion.7
  35.8 6.8 %all-to-all-start.1 = ((bf16[16,112,128]{2,1,0:T(8,128)(2,1)}), bf16[16,112,128]{2,1,0:T(8,128)(2,1)S(1)}, u32[]{:S(2)}, u32[]{:S(2)}) async-start(bf16[16,112,128]{2,1,0:T(8,128)(2,1)} %broadcast_in_dim.45), calls=%async_computation.1 | async-start | bytes 917504 | tf_op jit(solution)/shard_map/all_to_all | solution.py:20
  43.6 8.4 %all-to-all-done.1 = bf16[16,112,128]{2,1,0:T(8,128)(2,1)S(1)} async-done(((bf16[16,112,128]{2,1,0:T(8,128)(2,1)}), bf16[16,112,128]{2,1,0:T(8,128)(2,1)S(1)}, u32[]{:S(2)}, u32[]{:S(2)}) %all-to-all-start.1) | async-done | bytes 458784 | tf_op jit(solution)/shard_map/all_to_all | solution.py:20
  53.1 1.1 convolution_convert_fusion.1
  56.0 6.1 %all-to-all-start.2 = ((bf16[32,2,576]{2,1,0:T(2,128)(2,1)}), bf16[32,2,576]{2,1,0:T(2,128)(2,1)S(1)}, u32[]{:S(2)}, u32[]{:S(2)}) async-start(bf16[32,2,576]{2,1,0:T(2,128)(2,1)} %reshape.267), calls=%async_computation.2 | async-start | bytes 163840 | tf_op jit(solution)/shard_map/all_to_all | solution.py:20
  62.4 13.4 %all-to-all-done.2 = bf16[32,2,576]{2,1,0:T(2,128)(2,1)S(1)} async-done(((bf16[32,2,576]{2,1,0:T(2,128)(2,1)}), bf16[32,2,576]{2,1,0:T(2,128)(2,1)S(1)}, u32[]{:S(2)}, u32[]{:S(2)}) %all-to-all-start.2) | async-done | bytes 73760 | tf_op jit(solution)/shard_map/all_to_all | solution.py:20
  78.2 18.2 %all_to_all.50 = bf16[32,2,640]{2,1,0:T(2,128)(2,1)S(1)} all-to-all(bf16[32,2,640]{2,1,0:T(2,128)(2,1)S(1)} %copy.141), channel_id=1, replica_groups=mesh['kv_0'=4,'kv_1'=4,'tp'=32] {'tp'}, dimensions={0} | all-to-all | bytes 163840 | tf_op jit(solution)/shard_map/all_to_all | solution.py:20
  96.7 12.7 %all_to_all.51 = bf16[16,64,256]{2,1,0:T(8,128)(2,1)S(1)} all-to-all(bf16[16,64,256]{2,1,0:T(8,128)(2,1)S(1)} %broadcast_in_dim.51), channel_id=1, replica_groups=mesh['kv_0'=4,'kv_1'=4,'tp'=32] {'kv_0','kv_1'}, dimensions={0} | all-to-all | bytes 1048576 | tf_op jit(solution)/shard_map/all_to_all | solution.py:20
  109.4 1.3 fusion.74
  110.7 1.1 copy.166
  111.8 1.1 copy.167
  112.9 1.1 copy.168
  117.8 5.9 %all-to-all-start.5 = ((bf16[32,2,256]{2,1,0:T(2,128)(2,1)}), bf16[32,2,256]{2,1,0:T(2,128)(2,1)S(1)}, u32[]{:S(2)}, u32[]{:S(2)}) async-start(bf16[32,2,256]{2,1,0:T(2,128)(2,1)} %reshape.269), calls=%async_computation.5 | async-start | bytes 65536 | tf_op jit(solution)/shard_map/all_to_all | solution.py:20
  123.9 12.1 %all-to-all-done.5 = bf16[32,2,256]{2,1,0:T(2,128)(2,1)S(1)} async-done(((bf16[32,2,256]{2,1,0:T(2,128)(2,1)}), bf16[32,2,256]{2,1,0:T(2,128)(2,1)S(1)}, u32[]{:S(2)}, u32[]{:S(2)}) %all-to-all-start.5) | async-done | bytes 32800 | tf_op jit(solution)/shard_map/all_to_all | solution.py:20
  136.1 15.9 %all_to_all.52 = bf16[32,2,256]{2,1,0:T(2,128)(2,1)S(1)} all-to-all(bf16[32,2,256]{2,1,0:T(2,128)(2,1)S(1)} %broadcast_in_dim.52), channel_id=1, replica_groups=mesh['kv_0'=4,'kv_1'=4,'tp'=32] {'tp'}, dimensions={0} | all-to-all | bytes 65536 | tf_op jit(solution)/shard_map/all_to_all | solution.py:20
  153.0 1.1 convolution_convert_fusion
  154.3 9.3 %all_to_all.53 = bf16[16,4,640]{2,1,0:T(4,128)(2,1)S(1)} all-to-all(bf16[16,4,640]{2,1,0:T(4,128)(2,1)S(1)} %copy.152), channel_id=1, replica_groups=mesh['kv_0'=4,'kv_1'=4,'tp'=32] {'kv_0','kv_1'}, dimensions={0} | all-to-all | bytes 163840 | tf_op jit(solution)/shard_map/all_to_all | solution.py:20
  163.8 9.7 %all_to_all.54 = bf16[16,4,512]{2,1,0:T(4,128)(2,1)S(1)} all-to-all(bf16[16,4,512]{2,1,0:T(4,128)(2,1)S(1)} %broadcast_in_dim.55), channel_id=1, replica_groups=mesh['kv_0'=4,'kv_1'=4,'tp'=32] {'kv_0','kv_1'}, dimensions={0} | all-to-all | bytes 131072 | tf_op jit(solution)/shard_map/all_to_all | solution.py:20
  174.5 7.1 %all-to-all-start.9 = ((bf16[32,2,256]{2,1,0:T(2,128)(2,1)}), bf16[32,2,256]{2,1,0:T(2,128)(2,1)S(1)}, u32[]{:S(2)}, u32[]{:S(2)}) async-start(bf16[32,2,256]{2,1,0:T(2,128)(2,1)} %reshape.290), calls=%async_computation.9 | async-start | bytes 65536 | tf_op jit(solution)/shard_map/all_to_all | solution.py:20
  181.8 12.1 %all-to-all-done.9 = bf16[32,2,256]{2,1,0:T(2,128)(2,1)S(1)} async-done(((bf16[32,2,256]{2,1,0:T(2,128)(2,1)}), bf16[32,2,256]{2,1,0:T(2,128)(2,1)S(1)}, u32[]{:S(2)}, u32[]{:S(2)}) %all-to-all-start.9) | async-done | bytes 32800 | tf_op jit(solution)/shard_map/all_to_all | solution.py:20
  (120 shorter events, 21.4 us)
Async XLA Ops:
  0.0 76.0 %copy-start = (bf16[2,1024,512]{2,1,0:T(8,128)(2,1)S(1)}, bf16[2,1024,512]{2,1,0:T(8,128)(2,1)}, u32[]{:S(2)}) copy-start(bf16[2,1024,512]{2,1,0:T(8,128)(2,1)} %param.30) | copy-start | bytes 6291460
  0.0 34.6 %copy-start.3 = (bf16[256,128]{1,0:T(8,128)(2,1)S(1)}, bf16[256,128]{1,0:T(8,128)(2,1)}, u32[]{:S(2)}) copy-start(bf16[256,128]{1,0:T(8,128)(2,1)} %param.19) | copy-start | bytes 196612
  1.6 28.8 %all-to-all-start = ((bf16[32,2,256]{2,1,0:T(2,128)(2,1)}), bf16[32,2,256]{2,1,0:T(2,128)(2,1)S(1)}, u32[]{:S(2)}, u32[]{:S(2)}) async-start(bf16[32,2,256]{2,1,0:T(2,128)(2,1)} %reshape.288), calls=%async_computation | async-start | bytes 65536 | tf_op jit(solution)/shard_map/all_to_all | solution.py:20
  34.9 27.5 %copy-start.5 = (f32[512]{0:T(512)S(1)}, f32[512]{0:T(512)}, u32[]{:S(2)}) copy-start(f32[512]{0:T(512)} %param.23) | copy-start | bytes 6148
  35.8 16.3 %all-to-all-start.1 = ((bf16[16,112,128]{2,1,0:T(8,128)(2,1)}), bf16[16,112,128]{2,1,0:T(8,128)(2,1)S(1)}, u32[]{:S(2)}, u32[]{:S(2)}) async-start(bf16[16,112,128]{2,1,0:T(8,128)(2,1)} %broadcast_in_dim.45), calls=%async_computation.1 | async-start | bytes 917504 | tf_op jit(solution)/shard_map/all_to_all | solution.py:20
  56.0 19.9 %all-to-all-start.2 = ((bf16[32,2,576]{2,1,0:T(2,128)(2,1)}), bf16[32,2,576]{2,1,0:T(2,128)(2,1)S(1)}, u32[]{:S(2)}, u32[]{:S(2)}) async-start(bf16[32,2,576]{2,1,0:T(2,128)(2,1)} %reshape.267), calls=%async_computation.2 | async-start | bytes 163840 | tf_op jit(solution)/shard_map/all_to_all | solution.py:20
  76.9 19.6 %copy-start.2 = (bf16[512,128]{1,0:T(8,128)(2,1)S(1)}, bf16[512,128]{1,0:T(8,128)(2,1)}, u32[]{:S(2)}) copy-start(bf16[512,128]{1,0:T(8,128)(2,1)} %param.25) | copy-start | bytes 393220
  109.4 7.6 %copy-start.4 = (bf16[128,256]{1,0:T(8,128)(2,1)S(1)}, bf16[128,256]{1,0:T(8,128)(2,1)}, u32[]{:S(2)}) copy-start(bf16[128,256]{1,0:T(8,128)(2,1)} %param.26) | copy-start | bytes 196612
  114.2 59.2 %copy-start.1 = (bf16[512,256]{1,0:T(8,128)(2,1)S(1)}, bf16[512,256]{1,0:T(8,128)(2,1)}, u32[]{:S(2)}) copy-start(bf16[512,256]{1,0:T(8,128)(2,1)} %param.29) | copy-start | bytes 786436
  117.8 18.2 %all-to-all-start.5 = ((bf16[32,2,256]{2,1,0:T(2,128)(2,1)}), bf16[32,2,256]{2,1,0:T(2,128)(2,1)S(1)}, u32[]{:S(2)}, u32[]{:S(2)}) async-start(bf16[32,2,256]{2,1,0:T(2,128)(2,1)} %reshape.269), calls=%async_computation.5 | async-start | bytes 65536 | tf_op jit(solution)/shard_map/all_to_all | solution.py:20
  174.5 19.4 %all-to-all-start.9 = ((bf16[32,2,256]{2,1,0:T(2,128)(2,1)}), bf16[32,2,256]{2,1,0:T(2,128)(2,1)S(1)}, u32[]{:S(2)}, u32[]{:S(2)}) async-start(bf16[32,2,256]{2,1,0:T(2,128)(2,1)} %reshape.290), calls=%async_computation.9 | async-start | bytes 65536 | tf_op jit(solution)/shard_map/all_to_all | solution.py:20

commit v2 on v1

v2 whole, which is shorter than its diff:
```python
import jax
import jax.numpy as jnp
from jax import lax
from jax.experimental import pallas as pl
from jax.experimental.pallas import tpu as pltpu
from jax.sharding import Mesh
from jax.sharding import PartitionSpec as P

D = 4096
NOPE = 128
ROPE = 64
VD = 128
RANK = 512
LANE = 128
KV = ("kv_0", "kv_1")
KV_TP = ("kv_0", "kv_1", "tp")
EPS = 1e-06
BF = jnp.bfloat16
F32 = jnp.float32
NT = (((1,), (1,)), ((), ()))


def exchange(parts, axis):
    return lax.all_to_all(parts, axis, 0, 0, tiled=True)


def mm(a, b):
    return jnp.dot(a, b, preferred_element_type=F32)


def mm_nt(a, b):
    return lax.dot_general(a, b, NT, preferred_element_type=F32)


def split3(x):
    hi = x.astype(BF).astype(F32)
    rest = x - hi
    mid = rest.astype(BF).astype(F32)
    return hi, mid, rest - mid


def as_column(row):
    n = row.shape[1]
    full = jnp.broadcast_to(row, (LANE, n))
    return jnp.transpose(full)


def one_hot_rows(first, rows, columns):
    row = lax.broadcasted_iota(jnp.int32, (rows, columns), 0)
    column = lax.broadcasted_iota(jnp.int32, (rows, columns), 1)
    return jnp.where(column == first + row, 1.0, 0.0).astype(BF)


def read_pairs(ref, scratch):
    n, two, _ = ref.shape
    for i in range(n):
        scratch[two * i : two * (i + 1), :] = ref[i].astype(F32)
    return scratch[...]


def write_pairs(ref, scratch, value):
    n, two, _ = ref.shape
    scratch[...] = value
    for i in range(n):
        ref[i] = scratch[two * i : two * (i + 1), :].astype(BF)


def stage_query(at, got, gain, w_nope, w_rope, w_latent, w_key, out, own_out):
    n_tp, four, _ = got.shape
    seq_dev = own_out.shape[0]
    x = got[...].astype(F32)
    batch = LANE // 2
    block_t = jnp.concatenate([x[:, :, :batch], x[:, :, batch:]], axis=1)
    block_t = block_t.reshape(n_tp * 2 * four, batch)
    squares = jnp.sum(block_t * block_t, axis=0, keepdims=True)
    block = jnp.transpose(block_t)
    scaled = (block * gain[...]).astype(BF)
    nope = mm(scaled, w_nope[...])
    rope = mm(scaled, w_rope[...])
    pick = one_hot_rows(at[1] * seq_dev, 8, batch)
    own = mm(pick, scaled).astype(BF)
    own_out[...] = mm(pick, block.astype(BF))[:seq_dev]
    latent = mm(own, w_latent[...])
    key = mm(own, w_key[...])
    half = batch // 2
    rows = [
        nope,
        jnp.concatenate([rope[:half], rope[half:]], axis=1),
        *[latent[:2, LANE * j : LANE * (j + 1)] for j in range(RANK // LANE)],
        jnp.concatenate([key[0:1], key[1:2]], axis=1),
        jnp.concatenate([squares, squares], axis=1),
        jnp.zeros((6, LANE), F32),
    ]
    packed = jnp.concatenate(rows, axis=0).astype(BF)
    for j in range(out.shape[0]):
        out[j] = packed


def turned(values, cos_ref, sin_ref):
    half = values.shape[1] // 2
    swapped = jnp.concatenate([values[:, half:], values[:, :half]], axis=1)
    return values * cos_ref + swapped * sin_ref


def stage_absorb(at, got, w_key_up, gain_latent, cos_len, sin_len, out, new_out, scratch, trig):
    total = got[0].astype(F32)
    for j in range(1, got.shape[0]):
        total = total + got[j].astype(F32)
    batch = w_key_up.shape[1] // 2
    half = batch // 2
    nope = total[:batch]
    packed = total[batch : batch + half]
    rope = jnp.concatenate([packed[:, :ROPE], packed[:, ROPE:]], axis=0)
    at_row = batch + half
    latent = jnp.concatenate([total[at_row + 2 * j : at_row + 2 * j + 2] for j in range(4)], axis=1)
    key = total[at_row + 8 : at_row + 9]
    key = jnp.concatenate([key[:, :ROPE], key[:, ROPE:]], axis=0)
    squares = total[at_row + 9 : at_row + 10, :batch]
    inv = as_column(lax.rsqrt(squares / D + EPS))
    q_nope = (nope * inv).astype(BF)
    q_rope = turned(rope * inv[:, :ROPE], cos_len[...], sin_len[...])
    q_latent = mm_nt(q_nope, w_key_up[...])
    value = jnp.concatenate([q_latent, q_rope, jnp.zeros_like(q_rope)], axis=1)
    write_pairs(out, scratch, value)
    first = at[1] * 2
    trig[0] = inv
    trig[1] = jnp.concatenate([cos_len[...], sin_len[...]], axis=1)
    own_inv = trig[0, pl.ds(first, 2), :]
    own_trig = trig[1, pl.ds(first, 2), :]
    raw = latent * own_inv[:, :1]
    norm = lax.rsqrt(jnp.mean(raw * raw, axis=1, keepdims=True) + EPS)
    latent_new = raw * norm * gain_latent[...]
    key_new = turned(key * own_inv[:, :ROPE], own_trig[:, :ROPE], own_trig[:, ROPE:])
    new_out[...] = (
        jnp.concatenate([latent_new, key_new, jnp.zeros_like(key_new)], axis=1)
        .astype(BF)
        .astype(F32)
    )


def stage_attend(at, got, cache, rotated, new, out, scratch):
    query = read_pairs(got, scratch)
    rows = query.shape[0]
    cache_dev = cache.shape[1]
    latent_query = query[:, :RANK].astype(BF)
    rope_query = query[:, RANK : RANK + ROPE].astype(BF)
    even_column = lax.broadcasted_iota(jnp.int32, (rows, 1), 0) % 2 == 0
    scale = (NOPE + ROPE) ** (-0.5)
    each = [
        mm_nt(latent_query, cache[s]) + mm_nt(rope_query, rotated[s]) for s in range(2)
    ]
    scores = jnp.where(even_column, each[0], each[1]) * scale
    length = jnp.where(even_column, at[2], at[3])
    position = at[0] * cache_dev + lax.broadcasted_iota(jnp.int32, scores.shape, 1)
    live = position < length
    new_rows = jnp.where(even_column, new[0:1], new[1:2])
    own = jnp.sum(query * new_rows, axis=1, keepdims=True) * scale
    first = at[0] == 0
    peak = jnp.max(jnp.where(live, scores, -1e30), axis=1, keepdims=True)
    peak = jnp.where(first, jnp.maximum(peak, own), peak)
    expo = jnp.where(live, jnp.exp(scores - peak), 0.0)
    own_weight = jnp.where(first, jnp.exp(own - peak), 0.0)
    mass = jnp.sum(expo, axis=1, keepdims=True) + own_weight
    low = [
        jnp.where(even_column, expo, 0.0).astype(BF),
        jnp.where(even_column, 0.0, expo).astype(BF),
    ]
    weighted = mm(low[0], cache[0]) + mm(low[1], cache[1])
    weighted = weighted + own_weight * new_rows[:, :RANK]
    block_out = weighted / jnp.where(mass > 0, mass, 1.0)
    lane = lax.broadcasted_iota(jnp.int32, (rows, LANE), 1)
    stats = jnp.zeros((rows, LANE), F32)
    for i, piece in enumerate((*split3(peak), *split3(mass))):
        stats = jnp.where(lane == i, piece, stats)
    write_pairs(out, scratch, jnp.concatenate([block_out, stats], axis=1))


def stage_heads(got, w_value_up, out, scratch):
    value = read_pairs(got, scratch)
    part = mm(value[:, :RANK].astype(BF), w_value_up[...])
    stats = jnp.transpose(value[:, RANK:])[:16]
    stats = jnp.concatenate([stats, jnp.zeros_like(stats)], axis=1)
    packed = jnp.concatenate([part, stats], axis=0).astype(BF)
    for j in range(out.shape[0]):
        out[j] = packed


def stage_project(got, w_out, out, scratch):
    blocks, rows, _ = got.shape
    batch = rows - 16
    stats = got[:, batch:, :].astype(F32)
    peak = stats[:, 0] + (stats[:, 1] + stats[:, 2])
    mass = stats[:, 3] + (stats[:, 4] + stats[:, 5])
    top = jnp.max(peak, axis=0, keepdims=True)
    weight = mass * jnp.exp(peak - top)
    total = jnp.sum(weight, axis=0, keepdims=True)
    weight = weight / jnp.where(total > 0, total, 1.0)
    weight = jnp.concatenate([weight, jnp.zeros((LANE - blocks, LANE), F32)], axis=0)
    column = jnp.transpose(weight)[:batch]
    head = column[:, 0:1] * got[0, :batch].astype(F32)
    for j in range(1, blocks):
        head = head + column[:, j : j + 1] * got[j, :batch].astype(F32)
    write_pairs(out, scratch, mm(head.astype(BF), w_out[...]))


def stage_resid(got, own, out):
    total = own[...]
    for i in range(got.shape[0]):
        total = total + got[i].astype(F32)
    total = total.astype(BF)
    for i in range(out.shape[0]):
        out[i] = total


def stage_up(at, got, gain, w_up, out, own_out, scratch):
    resid = read_pairs(got, scratch)
    batch, width = resid.shape
    squares = jnp.sum(resid * resid, axis=1, keepdims=True)
    square_rows = jnp.transpose(jnp.broadcast_to(squares, (batch, LANE)))[:8]
    scaled = (resid * gain[...]).astype(BF)
    up = mm(scaled, w_up[...])
    units = up.shape[1]
    extra = jnp.concatenate([square_rows, jnp.zeros((8, units - batch), F32)], axis=1)
    packed = jnp.concatenate([up, extra], axis=0).astype(BF)
    for j in range(out.shape[0]):
        out[j] = packed
    pick = one_hot_rows(at[1] * 8, 8, width)
    own_out[...] = mm_nt(pick, resid.astype(BF))


def stage_down(got, w_down, out):
    total = got[0].astype(F32)
    for j in range(1, got.shape[0]):
        total = total + got[j].astype(F32)
    batch = total.shape[0] - 8
    active = jnp.square(jnp.maximum(total[:batch], 0.0)).astype(BF)
    inv = lax.rsqrt(total[batch : batch + 1, :batch] / D + EPS)
    down = jnp.transpose(mm(active, w_down[...])) * (inv * inv)
    n_tp = out.shape[0]
    down = down.reshape(n_tp, -1, batch)
    half = down.shape[1] // 2
    out[...] = jnp.concatenate([down[:, :half], down[:, half:]], axis=2).astype(BF)


def stage_last(got, own, out):
    total = jnp.sum(got[...].astype(F32), axis=0)
    batch = own.shape[1]
    value = jnp.concatenate([total[:, :batch], total[:, batch:]], axis=0) + own[...]
    value = jnp.concatenate([value, jnp.zeros_like(value)], axis=1)
    out[...] = jnp.transpose(value)[:batch].astype(BF)


def call(body, outs, operands, scratch=(), scalars=True):
    specs = [pl.BlockSpec(memory_space=pltpu.VMEM) for _ in operands]
    if scalars:
        specs[0] = pl.BlockSpec(memory_space=pltpu.SMEM)
    made = pl.pallas_call(
        body,
        out_shape=[jax.ShapeDtypeStruct(s, t) for s, t in outs],
        in_specs=specs,
        out_specs=[pl.BlockSpec(memory_space=pltpu.VMEM) for _ in outs],
        scratch_shapes=[pltpu.VMEM(s, F32) for s in scratch],
        name=body.__name__,
    )(*operands)
    return made if len(outs) > 1 else made[0]


def angles_of(positions):
    half_dim = ROPE // 2
    inv_freq = 10000.0 ** (-jnp.arange(half_dim, dtype=F32) / half_dim)
    angles = positions.astype(F32)[..., None] * inv_freq
    return jnp.cos(angles), jnp.sin(angles)


def per_device(
    tokens,
    lengths,
    gain_attn,
    w_query_nope,
    w_query_rope,
    w_latent,
    w_rope_key,
    gain_latent,
    w_key_up,
    w_value_up,
    w_out,
    gain_mlp,
    w_up,
    w_down,
    cache_latent,
    cache_rope,
):
    kv_index = lax.axis_index(KV)
    tp_index = lax.axis_index("tp")
    n_kv = lax.axis_size(KV)
    n_tp = lax.axis_size("tp")
    seq_dev, cache_dev = cache_latent.shape[:2]
    batch, out_cols = tokens.shape
    width = w_out.shape[1]
    units = w_up.shape[1]
    own_len = lax.dynamic_slice_in_dim(lengths, tp_index * seq_dev, seq_dev, 0)
    at = jnp.concatenate(
        [jnp.stack([kv_index, tp_index]).astype(jnp.int32), own_len.astype(jnp.int32)]
    )

    turned_tokens = tokens.T
    half = out_cols // 2
    sent = jnp.concatenate([turned_tokens[:half], turned_tokens[half:]], axis=1)
    got = exchange(jnp.broadcast_to(sent[None], (n_tp, half, LANE)), "tp")

    cos_len, sin_len = angles_of(lengths)
    cos_len = jnp.concatenate([cos_len, cos_len], axis=1)
    sin_len = jnp.concatenate([-sin_len, sin_len], axis=1)
    positions = kv_index * cache_dev + jnp.arange(cache_dev, dtype=jnp.int32)
    cos_pos, sin_pos = angles_of(positions)
    lower = cache_rope[..., : ROPE // 2].astype(F32)
    upper = cache_rope[..., ROPE // 2 :].astype(F32)
    rotated = jnp.concatenate(
        [lower * cos_pos - upper * sin_pos, upper * cos_pos + lower * sin_pos], axis=-1
    ).astype(BF)

    sent, own_tokens = call(
        stage_query,
        [((n_kv, 112, LANE), BF), ((seq_dev, width), F32)],
        [at, got, gain_attn[None], w_query_nope, w_query_rope, w_latent, w_rope_key],
    )
    got = exchange(sent, KV)
    sent, new = call(
        stage_absorb,
        [((n_tp, seq_dev, RANK + LANE), BF), ((seq_dev, RANK + LANE), F32)],
        [at, got, w_key_up, gain_latent[None], cos_len, sin_len],
        [(batch, RANK + LANE), (2, batch, LANE)],
    )
    got = exchange(sent, "tp")
    sent = call(
        stage_attend,
        [((n_tp, seq_dev, RANK + LANE), BF)],
        [at, got, cache_latent, rotated, new],
        [(batch, RANK + LANE)],
    )
    got = exchange(sent, "tp")
    sent = call(
        stage_heads,
        [((n_kv, batch + 16, LANE), BF)],
        [got, w_value_up],
        [(batch, RANK + LANE)],
        scalars=False,
    )
    got = exchange(sent, KV)
    sent = call(
        stage_project,
        [((n_tp, seq_dev, width), BF)],
        [got, w_out],
        [(batch, width)],
        scalars=False,
    )
    got = exchange(sent, "tp")
    sent = call(
        stage_resid, [((n_tp, seq_dev, width), BF)], [got, own_tokens], scalars=False
    )
    got = exchange(sent, "tp")
    sent, own_resid = call(
        stage_up,
        [((n_kv, batch + 8, units), BF), ((out_cols, batch), F32)],
        [at, got, gain_mlp[None], w_up],
        [(batch, width)],
    )
    got = exchange(sent, KV)
    sent = call(stage_down, [((n_tp, half, LANE), BF)], [got, w_down], scalars=False)
    got = exchange(sent, "tp")
    return call(stage_last, [((batch, out_cols), BF)], [got, own_resid], scalars=False)


def solution(mesh):
    split = Mesh(mesh.devices.reshape(4, 4, mesh.shape["tp"]), ("kv_0", "kv_1", "tp"))
    in_specs = (
        P(None, KV_TP),
        P(),
        P(KV),
        P(KV, "tp"),
        P(KV, "tp"),
        P(KV, None),
        P(KV, None),
        P(),
        P(None, "tp"),
        P(None, "tp"),
        P("tp", KV),
        P(KV),
        P(KV, "tp"),
        P("tp", KV),
        P("tp", KV, None),
        P("tp", KV, None),
    )
    out_specs = P(None, KV_TP)
    return jax.shard_map(
        per_device, mesh=split, in_specs=in_specs, out_specs=out_specs, check_vma=False
    )
```

time: 196 us -> 202 us (1.031)
  blocking collectives: 65.8 us -> 109 us
  waiting for transfers between devices: 54 us -> 24.3 us
  Pallas kernels: 0 us -> 19.8 us
  starting transfers between devices: 42.6 us -> 32.4 us
  matrix products: 7.78 us -> 0 us
  other arithmetic: 11.4 us -> 6.57 us
  local copies, waits for them, and re-layouts: 12.7 us -> 9.03 us
    all_to_all x5 -> x6, blocking collectives: 65.8 us -> 109 us  [exchange(): return lax.all_to_all(parts, axis, 0, 0, tiled=True)]
    all_to_all x5 -> x3, waiting for transfers between devices: 54 us -> 24.3 us  [exchange(): return lax.all_to_all(parts, axis, 0, 0, tiled=True)]
    pallas_call x0 -> x9, Pallas kernels: none -> 19.8 us  [call(): pl.pallas_call(body, out_shape=[jax.ShapeDtypeStruct(s, t) for s, t in ou...]
    all_to_all x5 -> x3, starting transfers between devices: 42.6 us -> 32.4 us  [exchange(): return lax.all_to_all(parts, axis, 0, 0, tiled=True)]
    dot_general x14 -> x0, matrix products: 7.78 us -> none  [the longest x1 1.2 us: per_device(): lax.dot_general(own_rows, w_latent, dims, preferred_element_type=F32)]
    convert_element_type x11 -> x3, other arithmetic: 5.19 us -> 1.66 us  [the longest x1 1 us: per_device(): lower = cache_rope[..., :ROPE // 2].astype(F32)]
    concatenate x4, other arithmetic: 0.19 us -> 2.51 us  [the longest x1 1.08 us: per_device(): jnp.concatenate([lower * cos_pos - upper * sin_pos, upper * cos_pos + low...]
    unnamed x25 -> x9, local copies, waits for them, and re-layouts: 6.43 us -> 5.22 us
  transfers between devices with their start and end apart: 5 -> 3, of which waited for: 5 -> 3; matrix products, arithmetic and copies ran while one was open for 3% -> 5% of each run, Pallas kernels for 0% -> 0%
where the time goes in v2:
time: 202 us; the launch traced here: 201 us
  blocking collectives  109 us (54%)
  starting transfers between devices  32.4 us (16%)
  waiting for transfers between devices  24.3 us (12%)
  Pallas kernels  19.8 us (10%)
  local copies, waits for them, and re-layouts  9.03 us (4%)
  other arithmetic  6.57 us (3%)
    all_to_all x6, blocking collectives, exchange(): return lax.all_to_all(parts, axis, 0, 0, tiled=True)  109 us
    all_to_all x3, starting transfers between devices, exchange(): return lax.all_to_all(parts, axis, 0, 0, tiled=True)  32.4 us
    all_to_all x3, waiting for transfers between devices, exchange(): return lax.all_to_all(parts, axis, 0, 0, tiled=True)  24.3 us
    pallas_call x9, Pallas kernels, call(): pl.pallas_call(body, out_shape=[jax.ShapeDtypeStruct(s, t) for s, t in ou...  19.8 us
    unnamed x9, local copies, waits for them, and re-layouts  5.22 us
  transfers between devices with their start and end apart: 3, of which 3 were waited for; matrix products, arithmetic and copies ran while one was open for 5% of the time, Pallas kernels for 0%

profile of v2, /device:TPU:1, one launch (start us, length us, event | category | flops | bytes accessed | tf_op | source)
XLA Modules:
  0.0 200.9 jit_solution(3996321498795146523)
XLA Ops:
  1.5 16.7 %all-to-all-start = ((bf16[32,4,128]{2,1,0:T(4,128)(2,1)}), bf16[32,4,128]{2,1,0:T(4,128)(2,1)S(1)}, u32[]{:S(2)}, u32[]{:S(2)}) async-start(bf16[32,4,128]{2,1,0:T(4,128)(2,1)} %broadcast_in_dim.8), calls=%async_computation | async-start | bytes 65536 | tf_op jit(solution)/shard_map/all_to_all | solution.py:24
  20.8 1.5 copy.22.w_rope
  22.3 1.5 copy.23.w_key
  25.0 5.2 %all-to-all-done.got = bf16[32,4,128]{2,1,0:T(4,128)(2,1)S(1)} async-done(((bf16[32,4,128]{2,1,0:T(4,128)(2,1)}), bf16[32,4,128]{2,1,0:T(4,128)(2,1)S(1)}, u32[]{:S(2)}, u32[]{:S(2)}) %all-to-all-start) | async-done | bytes 32800 | tf_op jit(solution)/shard_map/all_to_all | solution.py:24
  30.8 2.3 %stage_query.1 = (bf16[16,112,128]{2,1,0:T(8,128)(2,1)}, f32[2,256]{1,0:T(2,128)}) custom-call(s32[4]{0:T(128)} %pad_add_fusion.at, bf16[32,4,128]{2,1,0:T(4,128)(2,1)} %copy-done.2, f32[1,256]{1,0:T(1,128)} %bitcast.8, bf16[256,128]{1,0:T(8,128)(2,1)} %w_nope.1, bf16[256,64]{1,0:T(8,128)(2,1)} %copy.22.w_rope, bf16[256,512]{1,0:T(8,128)(2,1)} %w_latent.1, ...), custom_call_target="tpu_custom_call" | custom-call | tf_op jit(solution)/shard_map/stage_query/pallas_call | solution.py:257
  33.2 6.8 %all-to-all-start.1 = ((bf16[16,112,128]{2,1,0:T(8,128)(2,1)}), bf16[16,112,128]{2,1,0:T(8,128)(2,1)S(1)}, u32[]{:S(2)}, u32[]{:S(2)}) async-start(bf16[16,112,128]{2,1,0:T(8,128)(2,1)} %get-tuple-element.11), calls=%async_computation.1 | async-start | bytes 917504 | tf_op jit(solution)/shard_map/all_to_all | solution.py:24
  40.7 1.9 multiply_cosine_fusion
  42.5 6.8 %all-to-all-done.1.got = bf16[16,112,128]{2,1,0:T(8,128)(2,1)S(1)} async-done(((bf16[16,112,128]{2,1,0:T(8,128)(2,1)}), bf16[16,112,128]{2,1,0:T(8,128)(2,1)S(1)}, u32[]{:S(2)}, u32[]{:S(2)}) %all-to-all-start.1) | async-done | bytes 458784 | tf_op jit(solution)/shard_map/all_to_all | solution.py:24
  50.2 2.1 %stage_absorb.1 = (bf16[32,2,640]{2,1,0:T(2,128)(2,1)}, f32[2,640]{1,0:T(2,128)}) custom-call(s32[4]{0:T(128)} %pad_add_fusion.at, bf16[16,112,128]{2,1,0:T(8,128)(2,1)} %copy-done, bf16[512,128]{1,0:T(8,128)(2,1)} %w_key_up.1, f32[1,512]{1,0:T(1,128)} %bitcast.6, f32[64,64]{1,0:T(8,128)} %get-tuple-element.28.cos_len, f32[64,64]{1,0:T(8,128)} %get-tuple-element.29.sin_len), custom_call_target="tpu_custom_call" | custom-call | tf_op jit(solution)/shard_map/stage_absorb/pallas_call | solution.py:257
  52.2 8.9 %all-to-all-start.2 = ((bf16[32,2,640]{2,1,0:T(2,128)(2,1)}), bf16[32,2,640]{2,1,0:T(2,128)(2,1)S(1)}, u32[]{:S(2)}, u32[]{:S(2)}) async-start(bf16[32,2,640]{2,1,0:T(2,128)(2,1)} %get-tuple-element.12), calls=%async_computation.2 | async-start | bytes 163840 | tf_op jit(solution)/shard_map/all_to_all | solution.py:24
  62.5 12.3 %all-to-all-done.2.got = bf16[32,2,640]{2,1,0:T(2,128)(2,1)S(1)} async-done(((bf16[32,2,640]{2,1,0:T(2,128)(2,1)}), bf16[32,2,640]{2,1,0:T(2,128)(2,1)S(1)}, u32[]{:S(2)}, u32[]{:S(2)}) %all-to-all-start.2) | async-done | bytes 81952 | tf_op jit(solution)/shard_map/all_to_all | solution.py:24
  75.5 3.9 %stage_attend.1 = bf16[32,2,640]{2,1,0:T(2,128)(2,1)} custom-call(s32[4]{0:T(128)} %pad_add_fusion.at, bf16[32,2,640]{2,1,0:T(2,128)(2,1)} %copy-done.1, bf16[2,1024,512]{2,1,0:T(8,128)(2,1)} %cache.1, bf16[2,1024,64]{2,1,0:T(8,128)(2,1)} %pad_maximum_fusion.rotated, f32[2,640]{1,0:T(2,128)} %get-tuple-element.13.new), custom_call_target="tpu_custom_call" | custom-call | tf_op jit(solution)/shard_map/stage_attend/pallas_call | solution.py:257
  79.3 19.8 %all_to_all.45.got = bf16[32,2,640]{2,1,0:T(2,128)(2,1)} all-to-all(bf16[32,2,640]{2,1,0:T(2,128)(2,1)} %stage_attend.1), channel_id=1, replica_groups=mesh['kv_0'=4,'kv_1'=4,'tp'=32] {'tp'}, dimensions={0} | all-to-all | bytes 163840 | tf_op jit(solution)/shard_map/all_to_all | solution.py:24
  99.1 1.8 stage_heads.1
  101.0 12.3 %all_to_all.46.got = bf16[16,80,128]{2,1,0:T(8,128)(2,1)} all-to-all(bf16[16,80,128]{2,1,0:T(8,128)(2,1)} %stage_heads.1), channel_id=1, replica_groups=mesh['kv_0'=4,'kv_1'=4,'tp'=32] {'kv_0','kv_1'}, dimensions={0} | all-to-all | bytes 655360 | tf_op jit(solution)/shard_map/all_to_all | solution.py:24
  113.2 2.1 %stage_project.1 = bf16[32,2,256]{2,1,0:T(2,128)(2,1)} custom-call(bf16[16,80,128]{2,1,0:T(8,128)(2,1)} %all_to_all.46.got, bf16[128,256]{1,0:T(8,128)(2,1)} %w_out.1), custom_call_target="tpu_custom_call" | custom-call | tf_op jit(solution)/shard_map/stage_project/pallas_call | solution.py:257
  115.3 18.8 %all_to_all.47.got = bf16[32,2,256]{2,1,0:T(2,128)(2,1)} all-to-all(bf16[32,2,256]{2,1,0:T(2,128)(2,1)} %stage_project.1), channel_id=1, replica_groups=mesh['kv_0'=4,'kv_1'=4,'tp'=32] {'tp'}, dimensions={0} | all-to-all | bytes 65536 | tf_op jit(solution)/shard_map/all_to_all | solution.py:24
  134.1 1.4 stage_resid.1
  135.6 17.4 %all_to_all.48.got = bf16[32,2,256]{2,1,0:T(2,128)(2,1)} all-to-all(bf16[32,2,256]{2,1,0:T(2,128)(2,1)} %stage_resid.1), channel_id=1, replica_groups=mesh['kv_0'=4,'kv_1'=4,'tp'=32] {'tp'}, dimensions={0} | all-to-all | bytes 65536 | tf_op jit(solution)/shard_map/all_to_all | solution.py:24
  153.0 2.3 %stage_up.1 = (bf16[16,72,512]{2,1,0:T(8,128)(2,1)}, f32[8,64]{1,0:T(8,128)}) custom-call(s32[4]{0:T(128)} %pad_add_fusion.at, bf16[32,2,256]{2,1,0:T(2,128)(2,1)} %all_to_all.48.got, f32[1,256]{1,0:T(1,128)} %bitcast.9, bf16[256,512]{1,0:T(8,128)(2,1)} %w_up.1), custom_call_target="tpu_custom_call" | custom-call | tf_op jit(solution)/shard_map/stage_up/pallas_call | solution.py:257
  155.3 21.8 %all_to_all.49.got = bf16[16,72,512]{2,1,0:T(8,128)(2,1)} all-to-all(bf16[16,72,512]{2,1,0:T(8,128)(2,1)} %get-tuple-element.15), channel_id=1, replica_groups=mesh['kv_0'=4,'kv_1'=4,'tp'=32] {'kv_0','kv_1'}, dimensions={0} | all-to-all | bytes 2359296 | tf_op jit(solution)/shard_map/all_to_all | solution.py:24
  177.1 2.4 %stage_down.1 = bf16[32,4,128]{2,1,0:T(4,128)(2,1)} custom-call(bf16[16,72,512]{2,1,0:T(8,128)(2,1)} %all_to_all.49.got, bf16[512,256]{1,0:T(8,128)(2,1)} %w_down.1), custom_call_target="tpu_custom_call" | custom-call | tf_op jit(solution)/shard_map/stage_down/pallas_call | solution.py:257
  179.4 18.5 %all_to_all.50.got = bf16[32,4,128]{2,1,0:T(4,128)(2,1)} all-to-all(bf16[32,4,128]{2,1,0:T(4,128)(2,1)} %stage_down.1), channel_id=1, replica_groups=mesh['kv_0'=4,'kv_1'=4,'tp'=32] {'tp'}, dimensions={0} | all-to-all | bytes 65536 | tf_op jit(solution)/shard_map/all_to_all | solution.py:24
  198.0 1.5 stage_last.1
  (22 shorter events, 10.8 us)
Async XLA Ops:
  1.5 28.8 %all-to-all-start = ((bf16[32,4,128]{2,1,0:T(4,128)(2,1)}), bf16[32,4,128]{2,1,0:T(4,128)(2,1)S(1)}, u32[]{:S(2)}, u32[]{:S(2)}) async-start(bf16[32,4,128]{2,1,0:T(4,128)(2,1)} %broadcast_in_dim.8), calls=%async_computation | async-start | bytes 65536 | tf_op jit(solution)/shard_map/all_to_all | solution.py:24
  30.2 0.6 copy-start.2
  33.2 16.2 %all-to-all-start.1 = ((bf16[16,112,128]{2,1,0:T(8,128)(2,1)}), bf16[16,112,128]{2,1,0:T(8,128)(2,1)S(1)}, u32[]{:S(2)}, u32[]{:S(2)}) async-start(bf16[16,112,128]{2,1,0:T(8,128)(2,1)} %get-tuple-element.11), calls=%async_computation.1 | async-start | bytes 917504 | tf_op jit(solution)/shard_map/all_to_all | solution.py:24
  49.4 0.8 copy-start
  52.2 22.6 %all-to-all-start.2 = ((bf16[32,2,640]{2,1,0:T(2,128)(2,1)}), bf16[32,2,640]{2,1,0:T(2,128)(2,1)S(1)}, u32[]{:S(2)}, u32[]{:S(2)}) async-start(bf16[32,2,640]{2,1,0:T(2,128)(2,1)} %get-tuple-element.12), calls=%async_computation.2 | async-start | bytes 163840 | tf_op jit(solution)/shard_map/all_to_all | solution.py:24
  74.9 0.6 copy-start.1

commit v3 on v2

--- a/solution.py
+++ b/solution.py
@@ -45,6 +45,14 @@
     return jnp.transpose(full)
 
 
+def kv_at():
+    return lax.axis_index("kv_0") * lax.axis_size("kv_1") + lax.axis_index("kv_1")
+
+
+def tp_at():
+    return lax.axis_index("tp")
+
+
 def one_hot_rows(first, rows, columns):
     row = lax.broadcasted_iota(jnp.int32, (rows, columns), 0)
     column = lax.broadcasted_iota(jnp.int32, (rows, columns), 1)
@@ -65,7 +73,16 @@
         ref[i] = scratch[two * i : two * (i + 1), :].astype(BF)
 
 
-def stage_query(at, got, gain, w_nope, w_rope, w_latent, w_key, out, own_out):
+def stage_send(tokens_t, out):
+    x = tokens_t[...].astype(F32)
+    half = x.shape[0] // 2
+    packed = jnp.concatenate([x[:half], x[half:]], axis=1).astype(BF)
+    for j in range(out.shape[0]):
+        out[j] = packed
+
+
+def stage_query(got, gain, w_nope, w_rope_t, w_latent, w_key_t, cos_pos, cos_len, out, own_out):
+    del cos_pos, cos_len
     n_tp, four, _ = got.shape
     seq_dev = own_out.shape[0]
     x = got[...].astype(F32)
@@ -76,12 +93,12 @@
     block = jnp.transpose(block_t)
     scaled = (block * gain[...]).astype(BF)
     nope = mm(scaled, w_nope[...])
-    rope = mm(scaled, w_rope[...])
-    pick = one_hot_rows(at[1] * seq_dev, 8, batch)
+    rope = mm_nt(scaled, w_rope_t[...])
+    pick = one_hot_rows(tp_at() * seq_dev, 8, batch)
     own = mm(pick, scaled).astype(BF)
     own_out[...] = mm(pick, block.astype(BF))[:seq_dev]
     latent = mm(own, w_latent[...])
-    key = mm(own, w_key[...])
+    key = mm_nt(own, w_key_t[...])
     half = batch // 2
     rows = [
         nope,
@@ -102,7 +119,9 @@
     return values * cos_ref + swapped * sin_ref
 
 
-def stage_absorb(at, got, w_key_up, gain_latent, cos_len, sin_len, out, new_out, scratch, trig):
+def stage_absorb(got, w_key_up, gain_latent, cos_ref, sin_ref, out, new_out, scratch, trig):
+    cos_len = jnp.concatenate([cos_ref[...], cos_ref[...]], axis=1)
+    sin_len = jnp.concatenate([-sin_ref[...], sin_ref[...]], axis=1)
     total = got[0].astype(F32)
     for j in range(1, got.shape[0]):
         total = total + got[j].astype(F32)
@@ -118,13 +137,13 @@
     squares = total[at_row + 9 : at_row + 10, :batch]
     inv = as_column(lax.rsqrt(squares / D + EPS))
     q_nope = (nope * inv).astype(BF)
-    q_rope = turned(rope * inv[:, :ROPE], cos_len[...], sin_len[...])
+    q_rope = turned(rope * inv[:, :ROPE], cos_len, sin_len)
     q_latent = mm_nt(q_nope, w_key_up[...])
     value = jnp.concatenate([q_latent, q_rope, jnp.zeros_like(q_rope)], axis=1)
     write_pairs(out, scratch, value)
-    first = at[1] * 2
+    first = tp_at() * 2
     trig[0] = inv
-    trig[1] = jnp.concatenate([cos_len[...], sin_len[...]], axis=1)
+    trig[1] = jnp.concatenate([cos_len, sin_len], axis=1)
     own_inv = trig[0, pl.ds(first, 2), :]
     own_trig = trig[1, pl.ds(first, 2), :]
     raw = latent * own_inv[:, :1]
@@ -138,7 +157,7 @@
     )
 
 
-def stage_attend(at, got, cache, rotated, new, out, scratch):
+def stage_attend(lengths, got, cache, rope, cos_pos, sin_pos, new, out, scratch):
     query = read_pairs(got, scratch)
     rows = query.shape[0]
     cache_dev = cache.shape[1]
@@ -146,16 +165,26 @@
     rope_query = query[:, RANK : RANK + ROPE].astype(BF)
     even_column = lax.broadcasted_iota(jnp.int32, (rows, 1), 0) % 2 == 0
     scale = (NOPE + ROPE) ** (-0.5)
-    each = [
-        mm_nt(latent_query, cache[s]) + mm_nt(rope_query, rotated[s]) for s in range(2)
-    ]
+    half = ROPE // 2
+    each = []
+    for s in range(2):
+        lower = rope[s, :half].astype(F32)
+        upper = rope[s, half:].astype(F32)
+        rotated = jnp.concatenate(
+            [
+                lower * cos_pos[...] - upper * sin_pos[...],
+                upper * cos_pos[...] + lower * sin_pos[...],
+            ],
+            axis=0,
+        ).astype(BF)
+        each.append(mm_nt(latent_query, cache[s]) + mm(rope_query, rotated))
     scores = jnp.where(even_column, each[0], each[1]) * scale
-    length = jnp.where(even_column, at[2], at[3])
-    position = at[0] * cache_dev + lax.broadcasted_iota(jnp.int32, scores.shape, 1)
+    length = jnp.where(even_column, lengths[tp_at() * 2], lengths[tp_at() * 2 + 1])
+    position = kv_at() * cache_dev + lax.broadcasted_iota(jnp.int32, scores.shape, 1)
     live = position < length
     new_rows = jnp.where(even_column, new[0:1], new[1:2])
     own = jnp.sum(query * new_rows, axis=1, keepdims=True) * scale
-    first = at[0] == 0
+    first = kv_at() == 0
     peak = jnp.max(jnp.where(live, scores, -1e30), axis=1, keepdims=True)
     peak = jnp.where(first, jnp.maximum(peak, own), peak)
     expo = jnp.where(live, jnp.exp(scores - peak), 0.0)
@@ -212,7 +241,7 @@
         out[i] = total
 
 
-def stage_up(at, got, gain, w_up, out, own_out, scratch):
+def stage_up(got, gain, w_up, out, own_out, scratch):
     resid = read_pairs(got, scratch)
     batch, width = resid.shape
     squares = jnp.sum(resid * resid, axis=1, keepdims=True)
@@ -224,7 +253,7 @@
     packed = jnp.concatenate([up, extra], axis=0).astype(BF)
     for j in range(out.shape[0]):
         out[j] = packed
-    pick = one_hot_rows(at[1] * 8, 8, width)
+    pick = one_hot_rows(tp_at() * 8, 8, width)
     own_out[...] = mm_nt(pick, resid.astype(BF))
 
 
@@ -246,30 +275,28 @@
     total = jnp.sum(got[...].astype(F32), axis=0)
     batch = own.shape[1]
     value = jnp.concatenate([total[:, :batch], total[:, batch:]], axis=0) + own[...]
-    value = jnp.concatenate([value, jnp.zeros_like(value)], axis=1)
-    out[...] = jnp.transpose(value)[:batch].astype(BF)
-
-
-def call(body, outs, operands, scratch=(), scalars=True):
+    out[...] = value.astype(BF)
+
+
+def call(body, outs, operands, scratch=(), spaces=()):
     specs = [pl.BlockSpec(memory_space=pltpu.VMEM) for _ in operands]
-    if scalars:
-        specs[0] = pl.BlockSpec(memory_space=pltpu.SMEM)
+    for index, space in spaces:
+        specs[index] = pl.BlockSpec(memory_space=space)
     made = pl.pallas_call(
         body,
         out_shape=[jax.ShapeDtypeStruct(s, t) for s, t in outs],
         in_specs=specs,
         out_specs=[pl.BlockSpec(memory_space=pltpu.VMEM) for _ in outs],
         scratch_shapes=[pltpu.VMEM(s, F32) for s in scratch],
+        compiler_params=pltpu.CompilerParams(vmem_limit_bytes=16 * 1024 * 1024),
         name=body.__name__,
     )(*operands)
     return made if len(outs) > 1 else made[0]
 
 
-def angles_of(positions):
+def inv_freq():
     half_dim = ROPE // 2
-    inv_freq = 10000.0 ** (-jnp.arange(half_dim, dtype=F32) / half_dim)
-    angles = positions.astype(F32)[..., None] * inv_freq
-    return jnp.cos(angles), jnp.sin(angles)
+    return 10000.0 ** (-jnp.arange(half_dim, dtype=F32) / half_dim)
 
 
 def per_device(
@@ -291,52 +318,53 @@
     cache_rope,
 ):
     kv_index = lax.axis_index(KV)
-    tp_index = lax.axis_index("tp")
     n_kv = lax.axis_size(KV)
     n_tp = lax.axis_size("tp")
     seq_dev, cache_dev = cache_latent.shape[:2]
     batch, out_cols = tokens.shape
     width = w_out.shape[1]
     units = w_up.shape[1]
-    own_len = lax.dynamic_slice_in_dim(lengths, tp_index * seq_dev, seq_dev, 0)
-    at = jnp.concatenate(
-        [jnp.stack([kv_index, tp_index]).astype(jnp.int32), own_len.astype(jnp.int32)]
-    )
-
-    turned_tokens = tokens.T
     half = out_cols // 2
-    sent = jnp.concatenate([turned_tokens[:half], turned_tokens[half:]], axis=1)
-    got = exchange(jnp.broadcast_to(sent[None], (n_tp, half, LANE)), "tp")
-
-    cos_len, sin_len = angles_of(lengths)
-    cos_len = jnp.concatenate([cos_len, cos_len], axis=1)
-    sin_len = jnp.concatenate([-sin_len, sin_len], axis=1)
+
+    sent = call(stage_send, [((n_tp, half, LANE), BF)], [tokens.T])
+    got = exchange(sent, "tp")
+
+    angles = lengths.astype(F32)[:, None] * inv_freq()
+    cos_len, sin_len = jnp.cos(angles), jnp.sin(angles)
     positions = kv_index * cache_dev + jnp.arange(cache_dev, dtype=jnp.int32)
-    cos_pos, sin_pos = angles_of(positions)
-    lower = cache_rope[..., : ROPE // 2].astype(F32)
-    upper = cache_rope[..., ROPE // 2 :].astype(F32)
-    rotated = jnp.concatenate(
-        [lower * cos_pos - upper * sin_pos, upper * cos_pos + lower * sin_pos], axis=-1
-    ).astype(BF)
+    angles = positions.astype(F32)[None] * inv_freq()[:, None]
+    cos_pos, sin_pos = jnp.cos(angles), jnp.sin(angles)
+    any_space = pl.ANY
 
     sent, own_tokens = call(
         stage_query,
         [((n_kv, 112, LANE), BF), ((seq_dev, width), F32)],
-        [at, got, gain_attn[None], w_query_nope, w_query_rope, w_latent, w_rope_key],
+        [
+            got,
+            gain_attn[None],
+            w_query_nope,
+            w_query_rope.T,
+            w_latent,
+            w_rope_key.T,
+            cos_pos,
+            cos_len,
+        ],
+        spaces=[(6, any_space), (7, any_space)],
     )
     got = exchange(sent, KV)
     sent, new = call(
         stage_absorb,
         [((n_tp, seq_dev, RANK + LANE), BF), ((seq_dev, RANK + LANE), F32)],
-        [at, got, w_key_up, gain_latent[None], cos_len, sin_len],
+        [got, w_key_up, gain_latent[None], cos_len, sin_len],
         [(batch, RANK + LANE), (2, batch, LANE)],
     )
     got = exchange(sent, "tp")
     sent = call(
         stage_attend,
         [((n_tp, seq_dev, RANK + LANE), BF)],
-        [at, got, cache_latent, rotated, new],
+        [lengths, got, cache_latent, jnp.swapaxes(cache_rope, 1, 2), cos_pos, sin_pos, new],
         [(batch, RANK + LANE)],
+        [(0, pltpu.SMEM)],
     )
     got = exchange(sent, "tp")
     sent = call(
@@ -344,7 +372,6 @@
         [((n_kv, batch + 16, LANE), BF)],
         [got, w_value_up],
         [(batch, RANK + LANE)],
-        scalars=False,
     )
     got = exchange(sent, KV)
     sent = call(
@@ -352,23 +379,22 @@
         [((n_tp, seq_dev, width), BF)],
         [got, w_out],
         [(batch, width)],
-        scalars=False,
     )
     got = exchange(sent, "tp")
     sent = call(
-        stage_resid, [((n_tp, seq_dev, width), BF)], [got, own_tokens], scalars=False
+        stage_resid, [((n_tp, seq_dev, width), BF)], [got, own_tokens]
     )
     got = exchange(sent, "tp")
     sent, own_resid = call(
         stage_up,
         [((n_kv, batch + 8, units), BF), ((out_cols, batch), F32)],
-        [at, got, gain_mlp[None], w_up],
+        [got, gain_mlp[None], w_up],
         [(batch, width)],
     )
     got = exchange(sent, KV)
-    sent = call(stage_down, [((n_tp, half, LANE), BF)], [got, w_down], scalars=False)
-    got = exchange(sent, "tp")
-    return call(stage_last, [((batch, out_cols), BF)], [got, own_resid], scalars=False)
+    sent = call(stage_down, [((n_tp, half, LANE), BF)], [got, w_down])
+    got = exchange(sent, "tp")
+    return call(stage_last, [((out_cols, batch), BF)], [got, own_resid]).T
 
 
 def solution(mesh):

time: 202 us -> 174 us (0.86)
  blocking collectives: 109 us -> 134 us
  starting transfers between devices: 32.4 us -> 16.7 us
  Pallas kernels: 19.8 us -> 5.7 us
  waiting for transfers between devices: 24.3 us -> 10.6 us
  other arithmetic: 6.57 us -> 1.4 us
  local copies, waits for them, and re-layouts: 9.03 us -> 4.75 us
    all_to_all x6 -> x8, blocking collectives: 109 us -> 134 us  [exchange(): return lax.all_to_all(parts, axis, 0, 0, tiled=True)]
    all_to_all x3 -> x1, starting transfers between devices: 32.4 us -> 16.7 us  [exchange(): return lax.all_to_all(parts, axis, 0, 0, tiled=True)]
    pallas_call x9 -> x10, Pallas kernels: 19.8 us -> 5.7 us  [call(): pl.pallas_call(body, out_shape=[jax.ShapeDtypeStruct(s, t) for s, t in ou...]
    all_to_all x3 -> x1, waiting for transfers between devices: 24.3 us -> 10.6 us  [exchange(): return lax.all_to_all(parts, axis, 0, 0, tiled=True)]
    concatenate x4 -> x0, other arithmetic: 2.51 us -> none  [the longest x1 1.08 us: per_device(): jnp.concatenate([lower * cos_pos - upper * sin_pos, upper * cos_pos + low...]
    unnamed x9 -> x32, local copies, waits for them, and re-layouts: 5.22 us -> 4.75 us
  transfers between devices with their start and end apart: 3 -> 1, of which waited for: 3 -> 1; matrix products, arithmetic and copies ran while one was open for 5% -> 1% of each run, Pallas kernels for 0% -> 0%
where the time goes in v3:
time: 174 us
  blocking collectives  134 us (77%)
  starting transfers between devices  16.7 us (10%)
  waiting for transfers between devices  10.6 us (6%)
  Pallas kernels  5.7 us (3%)
  local copies, waits for them, and re-layouts  4.75 us (3%)
    all_to_all x8, blocking collectives, exchange(): return lax.all_to_all(parts, axis, 0, 0, tiled=True)  134 us
    all_to_all x1, starting transfers between devices, exchange(): return lax.all_to_all(parts, axis, 0, 0, tiled=True)  16.7 us
    all_to_all x1, waiting for transfers between devices, exchange(): return lax.all_to_all(parts, axis, 0, 0, tiled=True)  10.6 us
    pallas_call x10, Pallas kernels, call(): pl.pallas_call(body, out_shape=[jax.ShapeDtypeStruct(s, t) for s, t in ou...  5.7 us
    unnamed x32, local copies, waits for them, and re-layouts  4.75 us
  transfers between devices with their start and end apart: 1, of which 1 were waited for; matrix products, arithmetic and copies ran while one was open for 1% of the time, Pallas kernels for 0%

profile of v3, /device:TPU:1, one launch (start us, length us, event | category | flops | bytes accessed | tf_op | source)
XLA Modules:
  0.0 173.7 jit_solution(17329863055320322956)
XLA Ops:
  0.0 0.7 copy-done.12
  0.7 0.7 stage_send.1
  1.4 16.7 %all-to-all-start = ((bf16[32,4,128]{2,1,0:T(4,128)(2,1)}), bf16[32,4,128]{2,1,0:T(4,128)(2,1)S(1)}, u32[]{:S(2)}, u32[]{:S(2)}) async-start(bf16[32,4,128]{2,1,0:T(4,128)(2,1)} %stage_send.1), calls=%async_computation | async-start | bytes 65536 | tf_op jit(solution)/shard_map/all_to_all | solution.py:24
  18.2 0.7 convert_element_type.11
  18.8 0.5 multiply_sine_fusion
  19.6 10.6 %all-to-all-done.got = bf16[32,4,128]{2,1,0:T(4,128)(2,1)S(1)} async-done(((bf16[32,4,128]{2,1,0:T(4,128)(2,1)}), bf16[32,4,128]{2,1,0:T(4,128)(2,1)S(1)}, u32[]{:S(2)}, u32[]{:S(2)}) %all-to-all-start) | async-done | bytes 32800 | tf_op jit(solution)/shard_map/all_to_all | solution.py:24
  30.2 0.9 copy-done.2
  31.2 0.8 copy-done.7
  32.0 0.8 copy-done.9
  32.8 0.8 copy-done.10
  33.5 0.7 copy-done.13
  34.2 0.5 stage_query.1
  34.7 16.1 %all_to_all.45.got = bf16[16,112,128]{2,1,0:T(8,128)(2,1)S(1)} all-to-all(bf16[16,112,128]{2,1,0:T(8,128)(2,1)S(1)} %get-tuple-element.11), channel_id=1, replica_groups=mesh['kv_0'=4,'kv_1'=4,'tp'=32] {'kv_0','kv_1'}, dimensions={0} | all-to-all | bytes 917504 | tf_op jit(solution)/shard_map/all_to_all | solution.py:24
  51.1 18.8 %all_to_all.46.got = bf16[32,2,640]{2,1,0:T(2,128)(2,1)S(1)} all-to-all(bf16[32,2,640]{2,1,0:T(2,128)(2,1)S(1)} %get-tuple-element.12), channel_id=1, replica_groups=mesh['kv_0'=4,'kv_1'=4,'tp'=32] {'tp'}, dimensions={0} | all-to-all | bytes 163840 | tf_op jit(solution)/shard_map/all_to_all | solution.py:24
  70.0 2.0 %stage_attend.1 = bf16[32,2,640]{2,1,0:T(2,128)(2,1)S(1)} custom-call(s32[64]{0:T(128)S(1)} %copy-done.15, bf16[32,2,640]{2,1,0:T(2,128)(2,1)S(1)} %all_to_all.46.got, bf16[2,1024,512]{2,1,0:T(8,128)(2,1)S(1)} %copy-done, bf16[2,64,1024]{2,1,0:T(8,128)(2,1)S(1)} %bitcast.8, f32[32,1024]{1,0:T(8,128)S(1)} %get-tuple-element.18.cos_pos, ...), custom_call_target="tpu_custom_call" | custom-call | tf_op jit(solution)/shard_map/stage_attend/pallas_call | solution.py:285
  72.1 18.2 %all_to_all.47.got = bf16[32,2,640]{2,1,0:T(2,128)(2,1)S(1)} all-to-all(bf16[32,2,640]{2,1,0:T(2,128)(2,1)S(1)} %stage_attend.1), channel_id=1, replica_groups=mesh['kv_0'=4,'kv_1'=4,'tp'=32] {'tp'}, dimensions={0} | all-to-all | bytes 163840 | tf_op jit(solution)/shard_map/all_to_all | solution.py:24
  90.4 10.6 %all_to_all.48.got = bf16[16,80,128]{2,1,0:T(8,128)(2,1)S(1)} all-to-all(bf16[16,80,128]{2,1,0:T(8,128)(2,1)S(1)} %stage_heads.1), channel_id=1, replica_groups=mesh['kv_0'=4,'kv_1'=4,'tp'=32] {'kv_0','kv_1'}, dimensions={0} | all-to-all | bytes 655360 | tf_op jit(solution)/shard_map/all_to_all | solution.py:24
  101.0 0.5 stage_project.1
  101.5 17.7 %all_to_all.49.got = bf16[32,2,256]{2,1,0:T(2,128)(2,1)S(1)} all-to-all(bf16[32,2,256]{2,1,0:T(2,128)(2,1)S(1)} %stage_project.1), channel_id=1, replica_groups=mesh['kv_0'=4,'kv_1'=4,'tp'=32] {'tp'}, dimensions={0} | all-to-all | bytes 65536 | tf_op jit(solution)/shard_map/all_to_all | solution.py:24
  119.3 15.9 %all_to_all.50.got = bf16[32,2,256]{2,1,0:T(2,128)(2,1)S(1)} all-to-all(bf16[32,2,256]{2,1,0:T(2,128)(2,1)S(1)} %stage_resid.1), channel_id=1, replica_groups=mesh['kv_0'=4,'kv_1'=4,'tp'=32] {'tp'}, dimensions={0} | all-to-all | bytes 65536 | tf_op jit(solution)/shard_map/all_to_all | solution.py:24
  135.5 19.8 %all_to_all.51.got = bf16[16,72,512]{2,1,0:T(8,128)(2,1)S(1)} all-to-all(bf16[16,72,512]{2,1,0:T(8,128)(2,1)S(1)} %get-tuple-element.15), channel_id=1, replica_groups=mesh['kv_0'=4,'kv_1'=4,'tp'=32] {'kv_0','kv_1'}, dimensions={0} | all-to-all | bytes 2359296 | tf_op jit(solution)/shard_map/all_to_all | solution.py:24
  155.3 0.5 stage_down.1
  155.8 17.3 %all_to_all.52.got = bf16[32,4,128]{2,1,0:T(4,128)(2,1)S(1)} all-to-all(bf16[32,4,128]{2,1,0:T(4,128)(2,1)S(1)} %stage_down.1), channel_id=1, replica_groups=mesh['kv_0'=4,'kv_1'=4,'tp'=32] {'tp'}, dimensions={0} | all-to-all | bytes 65536 | tf_op jit(solution)/shard_map/all_to_all | solution.py:24
  173.0 0.7 stage_last.1
  (33 shorter events, 1.1 us)
Async XLA Ops:
  0.0 50.8 %copy-start.5 = (bf16[512,128]{1,0:T(8,128)(2,1)S(1)}, bf16[512,128]{1,0:T(8,128)(2,1)}, u32[]{:S(2)}) copy-start(bf16[512,128]{1,0:T(8,128)(2,1)} %w_key_up.1) | copy-start | bytes 393220
  0.0 50.8 %copy-start.11 = (f32[512]{0:T(512)S(1)}, f32[512]{0:T(512)}, u32[]{:S(2)}) copy-start(f32[512]{0:T(512)} %param.23) | copy-start | bytes 6148
  0.0 0.7 copy-start.12
  1.4 28.8 %all-to-all-start = ((bf16[32,4,128]{2,1,0:T(4,128)(2,1)}), bf16[32,4,128]{2,1,0:T(4,128)(2,1)S(1)}, u32[]{:S(2)}, u32[]{:S(2)}) async-start(bf16[32,4,128]{2,1,0:T(4,128)(2,1)} %stage_send.1), calls=%async_computation | async-start | bytes 65536 | tf_op jit(solution)/shard_map/all_to_all | solution.py:24
  18.8 51.1 %copy-start.4 = (bf16[2,1024,64]{1,2,0:T(8,128)(2,1)S(1)}, bf16[2,1024,64]{1,2,0:T(8,128)(2,1)}, u32[]{:S(2)}) copy-start(bf16[2,1024,64]{1,2,0:T(8,128)(2,1)} %param.31) | copy-start | bytes 786436
  19.4 50.6 %copy-start.15 = (s32[64]{0:T(128)S(1)}, s32[64]{0:T(128)}, u32[]{:S(2)}) copy-start(s32[64]{0:T(128)} %lengths.1) | copy-start | bytes 772
  19.6 50.4 %copy-start = (bf16[2,1024,512]{2,1,0:T(8,128)(2,1)S(1)}, bf16[2,1024,512]{2,1,0:T(8,128)(2,1)}, u32[]{:S(2)}) copy-start(bf16[2,1024,512]{2,1,0:T(8,128)(2,1)} %cache.1) | copy-start | bytes 6291460
  30.2 1.0 copy-start.2
  31.2 0.8 copy-start.7
  32.0 0.8 copy-start.9
  32.8 0.8 copy-start.10
  33.5 0.7 copy-start.13
  70.0 20.2 %copy-start.6 = (bf16[512,128]{1,0:T(8,128)(2,1)S(1)}, bf16[512,128]{1,0:T(8,128)(2,1)}, u32[]{:S(2)}) copy-start(bf16[512,128]{1,0:T(8,128)(2,1)} %w_value_up.1) | copy-start | bytes 393220
  72.0 29.0 %copy-start.8 = (bf16[128,256]{1,0:T(8,128)(2,1)S(1)}, bf16[128,256]{1,0:T(8,128)(2,1)}, u32[]{:S(2)}) copy-start(bf16[128,256]{1,0:T(8,128)(2,1)} %w_out.1) | copy-start | bytes 196612
  72.1 63.2 %copy-start.1 = (bf16[256,512]{1,0:T(8,128)(2,1)S(1)}, bf16[256,512]{1,0:T(8,128)(2,1)}, u32[]{:S(2)}) copy-start(bf16[256,512]{1,0:T(8,128)(2,1)} %w_up.1) | copy-start | bytes 786436
  72.1 63.2 %copy-start.14 = (f32[256]{0:T(256)S(1)}, f32[256]{0:T(256)}, u32[]{:S(2)}) copy-start(f32[256]{0:T(256)} %param.27) | copy-start | bytes 3076
  135.5 19.9 %copy-start.3 = (bf16[512,256]{1,0:T(8,128)(2,1)S(1)}, bf16[512,256]{1,0:T(8,128)(2,1)}, u32[]{:S(2)}) copy-start(bf16[512,256]{1,0:T(8,128)(2,1)} %w_down.1) | copy-start | bytes 786436

commit v4 on v3

--- a/solution.py
+++ b/solution.py
@@ -13,7 +13,8 @@
 RANK = 512
 LANE = 128
 KV = ("kv_0", "kv_1")
-KV_TP = ("kv_0", "kv_1", "tp")
+TP = ("far", "near")
+KV_TP = ("kv_0", "kv_1", "far", "near")
 EPS = 1e-06
 BF = jnp.bfloat16
 F32 = jnp.float32
@@ -50,7 +51,7 @@
 
 
 def tp_at():
-    return lax.axis_index("tp")
+    return lax.axis_index("far") * lax.axis_size("near") + lax.axis_index("near")
 
 
 def one_hot_rows(first, rows, columns):
@@ -84,7 +85,6 @@
 def stage_query(got, gain, w_nope, w_rope_t, w_latent, w_key_t, cos_pos, cos_len, out, own_out):
     del cos_pos, cos_len
     n_tp, four, _ = got.shape
-    seq_dev = own_out.shape[0]
     x = got[...].astype(F32)
     batch = LANE // 2
     block_t = jnp.concatenate([x[:, :, :batch], x[:, :, batch:]], axis=1)
@@ -94,9 +94,11 @@
     scaled = (block * gain[...]).astype(BF)
     nope = mm(scaled, w_nope[...])
     rope = mm_nt(scaled, w_rope_t[...])
-    pick = one_hot_rows(tp_at() * seq_dev, 8, batch)
-    own = mm(pick, scaled).astype(BF)
-    own_out[...] = mm(pick, block.astype(BF))[:seq_dev]
+    own = mm(one_hot_rows(tp_at() * 2, 8, batch), scaled).astype(BF)
+    rows = own_out.shape[0]
+    own_out[...] = mm(
+        one_hot_rows(lax.axis_index("near") * rows, rows, batch), block.astype(BF)
+    )
     latent = mm(own, w_latent[...])
     key = mm_nt(own, w_key_t[...])
     half = batch // 2
@@ -214,7 +216,7 @@
         out[j] = packed
 
 
-def stage_project(got, w_out, out, scratch):
+def stage_project(got, w_out, out):
     blocks, rows, _ = got.shape
     batch = rows - 16
     stats = got[:, batch:, :].astype(F32)
@@ -229,7 +231,17 @@
     head = column[:, 0:1] * got[0, :batch].astype(F32)
     for j in range(1, blocks):
         head = head + column[:, j : j + 1] * got[j, :batch].astype(F32)
-    write_pairs(out, scratch, mm(head.astype(BF), w_out[...]))
+    part = mm(head.astype(BF), w_out[...])
+    out[...] = part.reshape(out.shape).astype(BF)
+
+
+def stage_sum(got, out):
+    total = got[0].astype(F32)
+    for i in range(1, got.shape[0]):
+        total = total + got[i].astype(F32)
+    total = total.astype(BF)
+    for i in range(out.shape[0]):
+        out[i] = total
 
 
 def stage_resid(got, own, out):
@@ -241,8 +253,9 @@
         out[i] = total
 
 
-def stage_up(got, gain, w_up, out, own_out, scratch):
-    resid = read_pairs(got, scratch)
+def stage_up(got, gain, w_up, out, own_out):
+    groups, rows, width = got.shape
+    resid = got[...].astype(F32).reshape(groups * rows, width)
     batch, width = resid.shape
     squares = jnp.sum(resid * resid, axis=1, keepdims=True)
     square_rows = jnp.transpose(jnp.broadcast_to(squares, (batch, LANE)))[:8]
@@ -278,6 +291,9 @@
     out[...] = value.astype(BF)
 
 
+COST = pl.CostEstimate(flops=40_000_000_000, transcendentals=0, bytes_accessed=20_000_000)
+
+
 def call(body, outs, operands, scratch=(), spaces=()):
     specs = [pl.BlockSpec(memory_space=pltpu.VMEM) for _ in operands]
     for index, space in spaces:
@@ -289,6 +305,7 @@
         out_specs=[pl.BlockSpec(memory_space=pltpu.VMEM) for _ in outs],
         scratch_shapes=[pltpu.VMEM(s, F32) for s in scratch],
         compiler_params=pltpu.CompilerParams(vmem_limit_bytes=16 * 1024 * 1024),
+        cost_estimate=COST,
         name=body.__name__,
     )(*operands)
     return made if len(outs) > 1 else made[0]
@@ -319,7 +336,8 @@
 ):
     kv_index = lax.axis_index(KV)
     n_kv = lax.axis_size(KV)
-    n_tp = lax.axis_size("tp")
+    n_tp = lax.axis_size(TP)
+    n_near, n_far = lax.axis_size("near"), lax.axis_size("far")
     seq_dev, cache_dev = cache_latent.shape[:2]
     batch, out_cols = tokens.shape
     width = w_out.shape[1]
@@ -327,7 +345,7 @@
     half = out_cols // 2
 
     sent = call(stage_send, [((n_tp, half, LANE), BF)], [tokens.T])
-    got = exchange(sent, "tp")
+    got = exchange(sent, TP)
 
     angles = lengths.astype(F32)[:, None] * inv_freq()
     cos_len, sin_len = jnp.cos(angles), jnp.sin(angles)
@@ -338,7 +356,7 @@
 
     sent, own_tokens = call(
         stage_query,
-        [((n_kv, 112, LANE), BF), ((seq_dev, width), F32)],
+        [((n_kv, 112, LANE), BF), ((batch // n_near, width), F32)],
         [
             got,
             gain_attn[None],
@@ -358,7 +376,7 @@
         [got, w_key_up, gain_latent[None], cos_len, sin_len],
         [(batch, RANK + LANE), (2, batch, LANE)],
     )
-    got = exchange(sent, "tp")
+    got = exchange(sent, TP)
     sent = call(
         stage_attend,
         [((n_tp, seq_dev, RANK + LANE), BF)],
@@ -366,7 +384,7 @@
         [(batch, RANK + LANE)],
         [(0, pltpu.SMEM)],
     )
-    got = exchange(sent, "tp")
+    got = exchange(sent, TP)
     sent = call(
         stage_heads,
         [((n_kv, batch + 16, LANE), BF)],
@@ -376,46 +394,50 @@
     got = exchange(sent, KV)
     sent = call(
         stage_project,
-        [((n_tp, seq_dev, width), BF)],
+        [((n_near, batch // n_near, width), BF)],
         [got, w_out],
-        [(batch, width)],
-    )
-    got = exchange(sent, "tp")
-    sent = call(
-        stage_resid, [((n_tp, seq_dev, width), BF)], [got, own_tokens]
-    )
-    got = exchange(sent, "tp")
+    )
+    got = exchange(sent, "near")
+    sent = call(stage_sum, [((n_far, batch // n_near, width), BF)], [got])
+    got = exchange(sent, "far")
+    sent = call(stage_resid, [((n_near, batch // n_near, width), BF)], [got, own_tokens])
+    got = exchange(sent, "near")
+    n_0, n_1 = lax.axis_size("kv_0"), lax.axis_size("kv_1")
     sent, own_resid = call(
         stage_up,
-        [((n_kv, batch + 8, units), BF), ((out_cols, batch), F32)],
+        [((n_1, batch + 8, units), BF), ((out_cols, batch), F32)],
         [got, gain_mlp[None], w_up],
-        [(batch, width)],
-    )
-    got = exchange(sent, KV)
+    )
+    got = exchange(sent, "kv_1")
+    sent = call(stage_sum, [((n_0, batch + 8, units), BF)], [got])
+    got = exchange(sent, "kv_0")
     sent = call(stage_down, [((n_tp, half, LANE), BF)], [got, w_down])
-    got = exchange(sent, "tp")
+    got = exchange(sent, TP)
     return call(stage_last, [((out_cols, batch), BF)], [got, own_resid]).T
 
 
 def solution(mesh):
-    split = Mesh(mesh.devices.reshape(4, 4, mesh.shape["tp"]), ("kv_0", "kv_1", "tp"))
+    n_tp = mesh.shape["tp"]
+    split = Mesh(
+        mesh.devices.reshape(4, 4, n_tp // 4, 4), ("kv_0", "kv_1", "far", "near")
+    )
     in_specs = (
         P(None, KV_TP),
         P(),
         P(KV),
-        P(KV, "tp"),
-        P(KV, "tp"),
+        P(KV, TP),
+        P(KV, TP),
         P(KV, None),
         P(KV, None),
         P(),
-        P(None, "tp"),
-        P(None, "tp"),
-        P("tp", KV),
+        P(None, TP),
+        P(None, TP),
+        P(TP, KV),
         P(KV),
-        P(KV, "tp"),
-        P("tp", KV),
-        P("tp", KV, None),
-        P("tp", KV, None),
+        P(KV, TP),
+        P(TP, KV),
+        P(TP, KV, None),
+        P(TP, KV, None),
     )
     out_specs = P(None, KV_TP)
     return jax.shard_map(

time: 174 us -> 165 us (0.948)
  blocking collectives: 134 us -> 129 us
  local copies, waits for them, and re-layouts: 4.75 us -> 0.74 us
    all_to_all x8 -> x10, blocking collectives: 134 us -> 129 us  [exchange(): return lax.all_to_all(parts, axis, 0, 0, tiled=True)]
    unnamed x32, local copies, waits for them, and re-layouts: 4.75 us -> 0.74 us
    pallas_call x10 -> x12, Pallas kernels: 5.7 us -> 5.56 us  [call(): pl.pallas_call(body, out_shape=[jax.ShapeDtypeStruct(s, t) for s, t in ou...]
  transfers between devices with their start and end apart: 1 -> 1, of which waited for: 1 -> 1; matrix products, arithmetic and copies ran while one was open for 1% -> 0% of each run, Pallas kernels for 0% -> 0%
where the time goes in v4:
time: 165 us; the launch traced here: 164 us
  blocking collectives  129 us (78%)
  starting transfers between devices  16.7 us (10%)
  waiting for transfers between devices  11.3 us (7%)
  Pallas kernels  5.56 us (3%)
    all_to_all x10, blocking collectives, exchange(): return lax.all_to_all(parts, axis, 0, 0, tiled=True)  129 us
    all_to_all x1, starting transfers between devices, exchange(): return lax.all_to_all(parts, axis, 0, 0, tiled=True)  16.7 us
    all_to_all x1, waiting for transfers between devices, exchange(): return lax.all_to_all(parts, axis, 0, 0, tiled=True)  11.3 us
    pallas_call x12, Pallas kernels, call(): pl.pallas_call(body, out_shape=[jax.ShapeDtypeStruct(s, t) for s, t in ou...  5.56 us
  transfers between devices with their start and end apart: 1, of which 1 were waited for; matrix products, arithmetic and copies ran while one was open for 0% of the time, Pallas kernels for 0%

profile of v4, /device:TPU:1, one launch (start us, length us, event | category | flops | bytes accessed | tf_op | source)
XLA Modules:
  0.0 164.0 jit_solution(3095560293067587464)
XLA Ops:
  0.0 0.7 copy-done.11
  0.7 0.7 stage_send.1
  1.4 16.7 %all-to-all-start = ((bf16[32,4,128]{2,1,0:T(4,128)(2,1)}), bf16[32,4,128]{2,1,0:T(4,128)(2,1)S(1)}, u32[]{:S(2)}, u32[]{:S(2)}) async-start(bf16[32,4,128]{2,1,0:T(4,128)(2,1)} %stage_send.1), calls=%async_computation | async-start | bytes 65536 | tf_op jit(solution)/shard_map/all_to_all | solution.py:25
  18.2 0.5 multiply_sine_fusion
  18.7 0.2 multiply_sine_fusion.1
  18.9 11.3 %all-to-all-done.got = bf16[32,4,128]{2,1,0:T(4,128)(2,1)S(1)} async-done(((bf16[32,4,128]{2,1,0:T(4,128)(2,1)}), bf16[32,4,128]{2,1,0:T(4,128)(2,1)S(1)}, u32[]{:S(2)}, u32[]{:S(2)}) %all-to-all-start) | async-done | bytes 32800 | tf_op jit(solution)/shard_map/all_to_all | solution.py:25
  30.3 0.5 stage_query.1
  30.8 16.1 %all_to_all.55.got = bf16[16,112,128]{2,1,0:T(8,128)(2,1)S(1)} all-to-all(bf16[16,112,128]{2,1,0:T(8,128)(2,1)S(1)} %get-tuple-element.11), channel_id=1, replica_groups=mesh['kv_0'=4,'kv_1'=4,'far'=8,'near'=4] {'kv_0','kv_1'}, dimensions={0} | all-to-all | bytes 917504 | tf_op jit(solution)/shard_map/all_to_all | solution.py:25
  46.8 0.4 stage_absorb.1
  47.2 19.0 %all_to_all.56.got = bf16[32,2,640]{2,1,0:T(2,128)(2,1)S(1)} all-to-all(bf16[32,2,640]{2,1,0:T(2,128)(2,1)S(1)} %get-tuple-element.12), channel_id=1, replica_groups=mesh['kv_0'=4,'kv_1'=4,'far'=8,'near'=4] {'far','near'}, dimensions={0} | all-to-all | bytes 163840 | tf_op jit(solution)/shard_map/all_to_all | solution.py:25
  66.2 2.0 %stage_attend.1 = bf16[32,2,640]{2,1,0:T(2,128)(2,1)S(1)} custom-call(s32[64]{0:T(128)S(1)} %copy-done.15, bf16[32,2,640]{2,1,0:T(2,128)(2,1)S(1)} %all_to_all.56.got, bf16[2,1024,512]{2,1,0:T(8,128)(2,1)S(1)} %copy-done, bf16[2,64,1024]{2,1,0:T(8,128)(2,1)S(1)} %bitcast.8, f32[32,1024]{1,0:T(8,128)S(1)} %get-tuple-element.18.cos_pos, ...), custom_call_target="tpu_custom_call" | custom-call | flops 40000000000 | bytes 20000000 | tf_op jit(solution)/shard_map/stage_attend/pallas_call | solution.py:301
  68.3 18.0 %all_to_all.57.got = bf16[32,2,640]{2,1,0:T(2,128)(2,1)S(1)} all-to-all(bf16[32,2,640]{2,1,0:T(2,128)(2,1)S(1)} %stage_attend.1), channel_id=1, replica_groups=mesh['kv_0'=4,'kv_1'=4,'far'=8,'near'=4] {'far','near'}, dimensions={0} | all-to-all | bytes 163840 | tf_op jit(solution)/shard_map/all_to_all | solution.py:25
  86.3 0.2 stage_heads.1
  86.5 10.6 %all_to_all.58.got = bf16[16,80,128]{2,1,0:T(8,128)(2,1)S(1)} all-to-all(bf16[16,80,128]{2,1,0:T(8,128)(2,1)S(1)} %stage_heads.1), channel_id=1, replica_groups=mesh['kv_0'=4,'kv_1'=4,'far'=8,'near'=4] {'kv_0','kv_1'}, dimensions={0} | all-to-all | bytes 655360 | tf_op jit(solution)/shard_map/all_to_all | solution.py:25
  97.0 0.5 stage_project.1
  97.6 8.4 %all_to_all.59.got = bf16[4,16,256]{2,1,0:T(8,128)(2,1)S(1)} all-to-all(bf16[4,16,256]{2,1,0:T(8,128)(2,1)S(1)} %stage_project.1), channel_id=1, replica_groups=mesh['kv_0'=4,'kv_1'=4,'far'=8,'near'=4] {'near'}, dimensions={0} | all-to-all | bytes 65536 | tf_op jit(solution)/shard_map/all_to_all | solution.py:25
  105.9 14.6 %all_to_all.60.got = bf16[8,16,256]{2,1,0:T(8,128)(2,1)S(1)} all-to-all(bf16[8,16,256]{2,1,0:T(8,128)(2,1)S(1)} %stage_sum.2), channel_id=1, replica_groups=mesh['kv_0'=4,'kv_1'=4,'far'=8,'near'=4] {'far'}, dimensions={0} | all-to-all | bytes 131072 | tf_op jit(solution)/shard_map/all_to_all | solution.py:25
  120.6 7.6 %all_to_all.61.got = bf16[4,16,256]{2,1,0:T(8,128)(2,1)S(1)} all-to-all(bf16[4,16,256]{2,1,0:T(8,128)(2,1)S(1)} %stage_resid.1), channel_id=1, replica_groups=mesh['kv_0'=4,'kv_1'=4,'far'=8,'near'=4] {'near'}, dimensions={0} | all-to-all | bytes 65536 | tf_op jit(solution)/shard_map/all_to_all | solution.py:25
  128.2 0.2 stage_up.1
  128.4 8.4 %all_to_all.62.got = bf16[4,72,512]{2,1,0:T(8,128)(2,1)S(1)} all-to-all(bf16[4,72,512]{2,1,0:T(8,128)(2,1)S(1)} %get-tuple-element.15), channel_id=1, replica_groups=mesh['kv_0'=4,'kv_1'=4,'far'=8,'near'=4] {'kv_1'}, dimensions={0} | all-to-all | bytes 589824 | tf_op jit(solution)/shard_map/all_to_all | solution.py:25
  136.8 8.2 %all_to_all.63.got = bf16[4,72,512]{2,1,0:T(8,128)(2,1)S(1)} all-to-all(bf16[4,72,512]{2,1,0:T(8,128)(2,1)S(1)} %stage_sum.3), channel_id=1, replica_groups=mesh['kv_0'=4,'kv_1'=4,'far'=8,'near'=4] {'kv_0'}, dimensions={0} | all-to-all | bytes 589824 | tf_op jit(solution)/shard_map/all_to_all | solution.py:25
  145.0 0.3 stage_down.1
  145.4 18.0 %all_to_all.64.got = bf16[32,4,128]{2,1,0:T(4,128)(2,1)S(1)} all-to-all(bf16[32,4,128]{2,1,0:T(4,128)(2,1)S(1)} %stage_down.1), channel_id=1, replica_groups=mesh['kv_0'=4,'kv_1'=4,'far'=8,'near'=4] {'far','near'}, dimensions={0} | all-to-all | bytes 65536 | tf_op jit(solution)/shard_map/all_to_all | solution.py:25
  163.3 0.7 stage_last.1
  (37 shorter events, 0.1 us)
Async XLA Ops:
  0.0 0.7 copy-start.11
  0.7 17.5 %copy-start.15 = (s32[64]{0:T(128)S(1)}, s32[64]{0:T(128)}, u32[]{:S(2)}) copy-start(s32[64]{0:T(128)} %lengths.1) | copy-start | bytes 772
  0.7 29.5 %copy-start.1 = (bf16[256,512]{1,0:T(8,128)(2,1)S(1)}, bf16[256,512]{1,0:T(8,128)(2,1)}, u32[]{:S(2)}) copy-start(bf16[256,512]{1,0:T(8,128)(2,1)} %w_latent.1) | copy-start | bytes 786436
  0.7 29.5 %copy-start.7 = (bf16[256,128]{1,0:T(8,128)(2,1)S(1)}, bf16[256,128]{1,0:T(8,128)(2,1)}, u32[]{:S(2)}) copy-start(bf16[256,128]{1,0:T(8,128)(2,1)} %w_nope.1) | copy-start | bytes 196612
  0.7 29.5 %copy-start.9 = (bf16[256,64]{0,1:T(8,128)(2,1)S(1)}, bf16[256,64]{0,1:T(8,128)(2,1)}, u32[]{:S(2)}) copy-start(bf16[256,64]{0,1:T(8,128)(2,1)} %param.20) | copy-start | bytes 98308
  0.7 29.5 %copy-start.10 = (bf16[256,64]{0,1:T(8,128)(2,1)S(1)}, bf16[256,64]{0,1:T(8,128)(2,1)}, u32[]{:S(2)}) copy-start(bf16[256,64]{0,1:T(8,128)(2,1)} %param.22) | copy-start | bytes 98308
  0.7 29.5 %copy-start.13 = (f32[256]{0:T(256)S(1)}, f32[256]{0:T(256)}, u32[]{:S(2)}) copy-start(f32[256]{0:T(256)} %param.18) | copy-start | bytes 3076
  1.4 28.8 %all-to-all-start = ((bf16[32,4,128]{2,1,0:T(4,128)(2,1)}), bf16[32,4,128]{2,1,0:T(4,128)(2,1)S(1)}, u32[]{:S(2)}, u32[]{:S(2)}) async-start(bf16[32,4,128]{2,1,0:T(4,128)(2,1)} %stage_send.1), calls=%async_computation | async-start | bytes 65536 | tf_op jit(solution)/shard_map/all_to_all | solution.py:25
  30.2 16.6 %copy-start.5 = (bf16[512,128]{1,0:T(8,128)(2,1)S(1)}, bf16[512,128]{1,0:T(8,128)(2,1)}, u32[]{:S(2)}) copy-start(bf16[512,128]{1,0:T(8,128)(2,1)} %w_key_up.1) | copy-start | bytes 393220
  30.2 16.6 %copy-start.12 = (f32[512]{0:T(512)S(1)}, f32[512]{0:T(512)}, u32[]{:S(2)}) copy-start(f32[512]{0:T(512)} %param.23) | copy-start | bytes 6148
  46.8 19.4 %copy-start = (bf16[2,1024,512]{2,1,0:T(8,128)(2,1)S(1)}, bf16[2,1024,512]{2,1,0:T(8,128)(2,1)}, u32[]{:S(2)}) copy-start(bf16[2,1024,512]{2,1,0:T(8,128)(2,1)} %cache.1) | copy-start | bytes 6291460
  46.8 19.4 %copy-start.2 = (bf16[2,1024,64]{1,2,0:T(8,128)(2,1)S(1)}, bf16[2,1024,64]{1,2,0:T(8,128)(2,1)}, u32[]{:S(2)}) copy-start(bf16[2,1024,64]{1,2,0:T(8,128)(2,1)} %param.31) | copy-start | bytes 786436
  66.2 20.1 %copy-start.6 = (bf16[512,128]{1,0:T(8,128)(2,1)S(1)}, bf16[512,128]{1,0:T(8,128)(2,1)}, u32[]{:S(2)}) copy-start(bf16[512,128]{1,0:T(8,128)(2,1)} %w_value_up.1) | copy-start | bytes 393220
  86.3 10.8 %copy-start.8 = (bf16[128,256]{1,0:T(8,128)(2,1)S(1)}, bf16[128,256]{1,0:T(8,128)(2,1)}, u32[]{:S(2)}) copy-start(bf16[128,256]{1,0:T(8,128)(2,1)} %w_out.1) | copy-start | bytes 196612
  120.5 7.6 %copy-start.3 = (bf16[256,512]{1,0:T(8,128)(2,1)S(1)}, bf16[256,512]{1,0:T(8,128)(2,1)}, u32[]{:S(2)}) copy-start(bf16[256,512]{1,0:T(8,128)(2,1)} %w_up.1) | copy-start | bytes 786436
  120.5 7.6 %copy-start.14 = (f32[256]{0:T(256)S(1)}, f32[256]{0:T(256)}, u32[]{:S(2)}) copy-start(f32[256]{0:T(256)} %param.27) | copy-start | bytes 3076
  136.8 8.2 %copy-start.4 = (bf16[512,256]{1,0:T(8,128)(2,1)S(1)}, bf16[512,256]{1,0:T(8,128)(2,1)}, u32[]{:S(2)}) copy-start(bf16[512,256]{1,0:T(8,128)(2,1)} %w_down.1) | copy-start | bytes 786436
